TPU v7x, 32 devices: a whole 2x2x4 slice. The times are simulated.
32 devices in a mesh: sp: 8 (over z, y), tp: 4 (over x, core).
Axes of the slice: x: 2, y: 2, z: 4, core: 2. Of those that a mesh axis runs over, the one named last changes fastest.
Arguments:
- latent: bfloat16 [3072, 2048], P(('sp', 'tp')), may hold values from -6 to 6
- context: bfloat16 [512, 2048], P('sp'), may hold values from -6 to 6
- cond_latent: float32 [2048], replicated, may hold values from -6 to 6
- cond_context: float32 [2048], replicated, may hold values from -12 to 12
- shift_weight: bfloat16 [2048, 2048], P('sp', 'tp'), may hold values from -0.125 to 0.125
- scale_weight: bfloat16 [2048, 2048], P('sp', 'tp'), may hold values from -0.125 to 0.125
- gate_weight: bfloat16 [2048, 2048], P('sp', 'tp'), may hold values from -0.125 to 0.125
- query_weight: bfloat16 [2, 2048, 1024], P(None, None, 'tp'), may hold values from -1.3258252 to 1.3258252
- key_weight: bfloat16 [2, 2048, 1024], P(None, None, 'tp'), may hold values from -1.3258252 to 1.3258252
- value_weight: bfloat16 [2048, 2048], P(None, 'tp'), may hold values from -0.125 to 0.125
- out_weight: bfloat16 [2048, 2048], P('tp'), may hold values from -0.125 to 0.125
- lambda_heads: float32 [16], P('tp'), may hold values from 0.3 to 0.8
- out_gain: float32 [2048], P('tp'), may hold values from 0.1 to 1.9
Outputs:
- result: bfloat16 [3072, 2048], P(('sp', 'tp'))
All inputs are finite; a program needn't handle non-finite values.
Results may differ from a plain program's by a relative error of at most 0.02.
The roundings to bfloat16 on the way count: a program that leaves them out, or rounds other values in their place, can miss the bound.
Values may be sent and summed in bfloat16 or wider, within the bound.
A program may use at most 128 MiB of HBM per device.

v0:
```python
import functools

import jax
import jax.numpy as jnp
import numpy as np
from jax import lax
from jax.experimental import pallas as pl
from jax.experimental.pallas import tpu as pltpu
from jax.sharding import PartitionSpec as P

HEAD_DIM = 64
GRID_W = 64
VALUE_DIM = 128
LANES = 128

norm_eps = 1e-06
rope_theta = 10000.0
f32 = jnp.float32
bf16 = jnp.bfloat16
MESH = pl.DeviceIdType.MESH


def pick(total, limit, unit):
    best = unit
    for size in range(unit, limit + 1, unit):
        if total % size == 0:
            best = size
    return best


def body(
    n_sp,
    n_tp,
    lat,
    ctx,
    cond_l,
    cond_c,
    shift_w,
    scale_w,
    gate_w,
    lane_table,
    lam,
    gain,
    wq_hbm,
    wk_hbm,
    wv_hbm,
    wo_hbm,
    out,
    wq,
    wk,
    wv,
    wo,
    mod_part,
    mod_recv,
    mod_all,
    raw,
    hidden,
    cos_t,
    sin_t,
    q_send,
    kv_send,
    kvc_send,
    q_buf,
    kv_buf,
    scores,
    o_send,
    heads,
    pair_send,
    pair_recv,
    fin_send,
    fin_recv,
    own_sum,
    w_sem,
    loc_sem,
    mod1_s,
    mod1_r,
    mod2_s,
    mod2_r,
    raw_s,
    raw_r,
    fwd_s,
    fwd_r,
    q_s,
    q_r,
    kv_s,
    kv_r,
    kvc_s,
    kvc_r,
    rel_s,
    rel_r,
    relc_s,
    relc_r,
    o_s,
    o_r,
    pair_s,
    pair_r,
    fin_s,
    fin_r,
):
    own, width = lat.shape
    ctx_rows = ctx.shape[0]
    tok = own * n_tp
    mod_cols = shift_w.shape[1]
    groups = q_send.shape[0]
    ranks = n_sp // groups
    chips = n_tp // 2
    sp_i = lax.axis_index("sp")
    tp_i = lax.axis_index("tp")
    g_i = sp_i // ranks
    r_i = sp_i % ranks
    chip_i = tp_i // 2
    core_i = tp_i % 2
    partner = chip_i * 2 + (1 - core_i)
    pending = []

    def send(src, dst, s_sem, r_sem, **where):
        copy = pltpu.make_async_remote_copy(
            src_ref=src, dst_ref=dst, send_sem=s_sem, recv_sem=r_sem,
            device_id=where, device_id_type=MESH,
        )
        copy.start()
        pending.append(copy)

    def arrived(ref, s_sem, r_sem, **where):
        pltpu.make_async_remote_copy(
            src_ref=ref, dst_ref=ref, send_sem=s_sem, recv_sem=r_sem,
            device_id=where, device_id_type=MESH,
        ).wait_recv()

    loads = [
        pltpu.make_async_copy(src, dst, w_sem.at[i])
        for i, (src, dst) in enumerate(
            ((wk_hbm, wk), (wv_hbm, wv), (wq_hbm, wq), (wo_hbm, wo))
        )
    ]
    for load in loads:
        load.start()

    barrier = pltpu.get_barrier_semaphore()
    for k in range(1, n_sp):
        pl.semaphore_signal(
            barrier, inc=1, device_id={"sp": (sp_i + k) % n_sp}, device_id_type=MESH
        )
    for k in range(1, n_tp):
        pl.semaphore_signal(
            barrier, inc=1, device_id={"tp": (tp_i + k) % n_tp}, device_id_type=MESH
        )

    def silu(v):
        return (v / (1.0 + jnp.exp(-v))).astype(bf16).astype(f32)

    c0 = silu(cond_l[sp_i])
    c1 = silu(cond_c[sp_i])
    row = lax.broadcasted_iota(jnp.int32, (8, c0.shape[-1]), 0)

    def placed_rows(at0, at1):
        zero = jnp.zeros(row.shape, f32)
        rows = jnp.where(row == at0, jnp.broadcast_to(c0, row.shape), zero)
        if at1 is not None:
            rows = jnp.where(row == at1, jnp.broadcast_to(c1, row.shape), rows)
        return rows.astype(bf16)

    mod_part[...] = (
        jnp.dot(placed_rows(0, 1), shift_w[...], preferred_element_type=f32)
        + jnp.dot(placed_rows(2, 3), scale_w[...], preferred_element_type=f32)
        + jnp.dot(placed_rows(4, None), gate_w[...], preferred_element_type=f32)
    )
    pl.semaphore_wait(barrier, n_sp + n_tp - 2)

    for k in range(1, n_sp):
        send(
            mod_part, mod_recv.at[sp_i], mod1_s.at[k], mod1_r.at[sp_i], sp=(sp_i + k) % n_sp
        )
    pieces = raw_s.shape[1]
    piece_rows = own // pieces

    def raw_piece(slot, i):
        return raw.at[slot, pl.ds(i * piece_rows, piece_rows)]

    def send_raw(i):
        for k in range(1, chips):
            send(
                lat.at[pl.ds(i * piece_rows, piece_rows)], raw_piece(tp_i, i),
                raw_s.at[k, i], raw_r.at[chip_i, i],
                tp=((chip_i + k) % chips) * 2 + core_i,
            )

    def relay_raw(i):
        for k in range(1, chips):
            src_chip = (chip_i + chips - k) % chips
            slot = src_chip * 2 + core_i
            arrived(raw_piece(slot, i), raw_s.at[k, i], raw_r.at[src_chip, i], tp=slot)
            send(
                raw_piece(slot, i), raw_piece(slot, i), fwd_s.at[k, i], fwd_r.at[src_chip, i],
                tp=partner,
            )

    early = max(pieces - 1, 1)
    for i in range(early):
        send_raw(i)
    send(lat, raw.at[tp_i], fwd_s.at[0, 0], fwd_r.at[chip_i, 0], tp=partner)
    raw[tp_i] = lat[...]
    mod_recv[sp_i] = mod_part[...]

    tok_row = lax.broadcasted_iota(jnp.int32, (tok, LANES), 0) + sp_i * tok
    grid_row = (tok_row // GRID_W).astype(f32)
    grid_col = (tok_row % GRID_W).astype(f32)
    angles = grid_row * lane_table[0:1, :] + grid_col * lane_table[1:2, :]
    cos_t[...] = jnp.cos(angles)
    sin_t[...] = jnp.sin(angles) * lane_table[2:3, :]

    for k in range(1, n_sp):
        src = (sp_i + n_sp - k) % n_sp
        arrived(mod_recv.at[src], mod1_s.at[k], mod1_r.at[src], sp=src)
    total = mod_recv[0]
    for s in range(1, n_sp):
        total = total + mod_recv[s]
    mod_part2 = mod_all.at[tp_i]
    mod_part2[...] = total
    for k in range(1, n_tp):
        send(
            mod_part2, mod_all.at[tp_i], mod2_s.at[k], mod2_r.at[tp_i], tp=(tp_i + k) % n_tp
        )
    for i in range(early, pieces):
        send_raw(i)
    for i in range(early):
        relay_raw(i)
    for k in range(1, n_tp):
        src = (tp_i + n_tp - k) % n_tp
        arrived(mod_all.at[src], mod2_s.at[k], mod2_r.at[src], tp=src)

    def modulate(x, which, start):
        at = pl.ds(start if isinstance(start, int) else pl.multiple_of(start, 16), x.shape[0])
        factor = lax.rsqrt(jnp.mean(x * x, axis=-1, keepdims=True) + norm_eps)
        for t in range(n_tp):
            cols = slice(t * mod_cols, (t + 1) * mod_cols)
            shift = mod_all[t, which : which + 1, :]
            scale = mod_all[t, which + 2 : which + 3, :]
            hidden[at, cols] = (
                (x[:, cols] * factor) * (1.0 + scale) + shift
            ).astype(bf16)

    half = 2 * own
    lane = lax.broadcasted_iota(jnp.int32, (half, LANES), 1)
    first_quarter = lane % HEAD_DIM < HEAD_DIM // 2
    low_half = lane < HEAD_DIM
    ctx_half = lax.broadcasted_iota(jnp.int32, (ctx_rows, LANES), 1) < HEAD_DIM

    def rope(u, rows):
        swapped = jnp.where(
            first_quarter,
            pltpu.roll(u, LANES - HEAD_DIM // 2, 1),
            pltpu.roll(u, HEAD_DIM // 2, 1),
        )
        return u * cos_t[rows, :] + swapped * sin_t[rows, :]

    def pair_up(a, b, low):
        return (
            jnp.where(low, a, pltpu.roll(b, HEAD_DIM, 1)).astype(bf16),
            jnp.where(low, pltpu.roll(a, HEAD_DIM, 1), b).astype(bf16),
        )

    def lat_slot(s, chip=None):
        if chip is None:
            return kv_buf.at[pl.ds(pl.multiple_of(s * tok, 16), tok)]
        return kv_buf.at[pl.ds(pl.multiple_of(s * tok + chip * half, 16), half)]

    def ctx_slot(s):
        return kv_buf.at[pl.ds(pl.multiple_of(n_sp * tok + s * ctx_rows, 16), ctx_rows)]

    order = list(range(1, groups))
    for c in range(chips):
        chip = (chip_i + c) % chips
        rows = pl.ds(pl.multiple_of(chip * half, 16), half)
        if c == 0:
            modulate(ctx[...].astype(f32), 1, half)
            modulate(raw[tp_i].astype(f32), 0, core_i * own)
            arrived(raw.at[partner], fwd_s.at[0, 0], fwd_r.at[chip_i, 0], tp=partner)
            modulate(raw[partner].astype(f32), 0, (1 - core_i) * own)
            for i in range(early, pieces):
                relay_raw(i)
            count = half + ctx_rows
        else:
            slot = chip * 2 + core_i
            modulate(raw[slot].astype(f32), 0, core_i * own)
            slot = chip * 2 + (1 - core_i)
            for i in range(pieces):
                arrived(
                    raw_piece(slot, i), fwd_s.at[chips - c, i], fwd_r.at[chip, i], tp=partner
                )
            modulate(raw[slot].astype(f32), 0, (1 - core_i) * own)
            count = half
        if c == 0:
            loads[0].wait()
        keys = [jnp.dot(hidden[:count, :], wk[m], preferred_element_type=f32) for m in (0, 1)]
        for p in range(groups // 2):
            slab = slice(p * LANES, (p + 1) * LANES)
            a, b = pair_up(
                rope(keys[0][:half, slab], rows), rope(keys[1][:half, slab], rows), low_half
            )
            kv_send[2 * p, rows, :LANES] = a
            kv_send[2 * p + 1, rows, :LANES] = b
            if c == 0:
                a, b = pair_up(keys[0][half:, slab], keys[1][half:, slab], ctx_half)
                kvc_send[2 * p, :, :LANES] = a
                kvc_send[2 * p + 1, :, :LANES] = b
        if c == 0:
            loads[1].wait()
        vals = jnp.dot(hidden[:count, :], wv[...], preferred_element_type=f32).astype(bf16)
        for j in range(groups):
            slab = slice(j * LANES, (j + 1) * LANES)
            kv_send[j, rows, LANES:] = vals[:half, slab]
            if c == 0:
                kvc_send[j, :, LANES:] = vals[half:, slab]
        for k in order:
            g = (g_i + k) % groups
            to = g * ranks + r_i
            send(
                kv_send.at[g, rows], lat_slot(sp_i, chip), kv_s.at[k, c], kv_r.at[g_i, c], sp=to
            )
            if c == 0:
                send(kvc_send.at[g], ctx_slot(sp_i), kvc_s.at[k], kvc_r.at[g_i], sp=to)
        for e in range(1, ranks):
            to = g_i * ranks + (r_i + e) % ranks
            send(
                kv_send.at[g_i, rows], lat_slot(sp_i, chip), rel_s.at[0, c, e],
                rel_r.at[g_i, c, r_i], sp=to,
            )
            if c == 0:
                send(
                    kvc_send.at[g_i], ctx_slot(sp_i), relc_s.at[0, e], relc_r.at[g_i, r_i], sp=to
                )
        if c == 0:
            loads[2].wait()
        queries = [
            jnp.dot(hidden[:half, :], wq[m], preferred_element_type=f32) for m in (0, 1)
        ]
        for p in range(groups // 2):
            slab = slice(p * LANES, (p + 1) * LANES)
            a, b = pair_up(
                rope(queries[0][:, slab], rows), rope(queries[1][:, slab], rows), low_half
            )
            q_send[2 * p, rows, :] = a
            q_send[2 * p + 1, rows, :] = b
    for k in order:
        g = (g_i + k) % groups
        send(q_send.at[g], q_buf.at[g_i], q_s.at[k], q_r.at[g_i], sp=g * ranks + r_i)
    local = [
        pltpu.make_async_copy(kv_send.at[g_i], lat_slot(sp_i), loc_sem.at[0]),
        pltpu.make_async_copy(kvc_send.at[g_i], ctx_slot(sp_i), loc_sem.at[1]),
        pltpu.make_async_copy(q_send.at[g_i], q_buf.at[g_i], loc_sem.at[2]),
    ]
    for copy in local:
        copy.start()

    for c in range(chips):
        chip = (chip_i + c) % chips
        for k in order:
            g = (g_i + groups - k) % groups
            s = g * ranks + r_i
            arrived(lat_slot(s, chip), kv_s.at[k, c], kv_r.at[g, c], sp=s)
            for e in range(1, ranks):
                to = g_i * ranks + (r_i + e) % ranks
                send(
                    lat_slot(s, chip), lat_slot(s, chip), rel_s.at[k, c, e],
                    rel_r.at[g, c, r_i], sp=to,
                )
            if c == 0:
                arrived(ctx_slot(s), kvc_s.at[k], kvc_r.at[g], sp=s)
                for e in range(1, ranks):
                    to = g_i * ranks + (r_i + e) % ranks
                    send(
                        ctx_slot(s), ctx_slot(s), relc_s.at[k, e], relc_r.at[g, r_i], sp=to
                    )
    for copy in local:
        copy.wait()
    for e in range(1, ranks):
        r = (r_i + ranks - e) % ranks
        to = g_i * ranks + r
        for k in range(groups):
            g = (g_i + groups - k) % groups
            s = g * ranks + r
            for c in range(chips):
                chip = (chip_i + c) % chips
                arrived(lat_slot(s, chip), rel_s.at[k, c, e], rel_r.at[g, c, r], sp=to)
            arrived(ctx_slot(s), relc_s.at[k, e], relc_r.at[g, r], sp=to)

    key_total = kv_buf.shape[0]
    q_tile = scores.shape[0] // 2
    block = pick(key_total, 512, LANES)
    coef = HEAD_DIM ** (-0.5) * 1.4426950408889634
    q_low = lax.broadcasted_iota(jnp.int32, (q_tile, LANES), 1) < HEAD_DIM
    head_lam = lam[g_i]
    tiles = tok // q_tile
    head_gain = gain[g_i]

    def attend(g, start):
        q = q_buf[g, pl.ds(start, q_tile), :]
        zero = jnp.zeros_like(q)
        q2 = jnp.concatenate([jnp.where(q_low, q, zero), jnp.where(q_low, zero, q)], axis=0)
        peak = None
        for b in range(key_total // block):
            rows = slice(b * block, (b + 1) * block)
            s = lax.dot_general(
                q2, kv_buf[rows, :LANES], (((1,), (1,)), ((), ())), preferred_element_type=f32
            )
            scores[:, rows] = s
            for c in range(block // LANES):
                piece = s[:, c * LANES : (c + 1) * LANES]
                peak = piece if peak is None else jnp.maximum(peak, piece)
        top = jnp.max(peak, axis=-1, keepdims=True) * coef
        sums = None
        acc = None
        for b in range(key_total // block):
            rows = slice(b * block, (b + 1) * block)
            w = jnp.exp2(scores[:, rows] * coef - top)
            for c in range(block // LANES):
                piece = w[:, c * LANES : (c + 1) * LANES]
                sums = piece if sums is None else sums + piece
            part = jnp.dot(w.astype(bf16), kv_buf[rows, LANES:], preferred_element_type=f32)
            acc = part if acc is None else acc + part
        mean_v = acc / jnp.sum(sums, axis=-1, keepdims=True)
        mixed = mean_v[:q_tile] - head_lam * mean_v[q_tile:]
        factor = lax.rsqrt(jnp.mean(mixed * mixed, axis=-1, keepdims=True) + norm_eps)
        o_send[g, pl.ds(start, q_tile), :] = (mixed * factor * head_gain).astype(bf16)

    def o_copy(k, i):
        g = (g_i + groups - k) % groups
        rows = pl.ds(pl.multiple_of(i * q_tile, 16), q_tile)
        return pltpu.make_async_remote_copy(
            src_ref=o_send.at[g, rows], dst_ref=heads.at[g_i, rows], send_sem=o_s.at[k, i],
            recv_sem=o_r.at[g_i, i], device_id={"sp": g * ranks + r_i}, device_id_type=MESH,
        )

    @pl.loop(0, groups)
    def _(k):
        g = (g_i + groups - k) % groups

        @pl.when(k > 0)
        def _():
            arrived(q_buf.at[g], q_s.at[k], q_r.at[g], sp=g * ranks + r_i)

        @pl.loop(0, tiles)
        def _(i):
            attend(g, pl.multiple_of(i * q_tile, q_tile))

            @pl.when(k > 0)
            def _():
                o_copy(k, i).start()

    heads[g_i] = o_send[g_i]
    loads[3].wait()
    for k in order:
        src = (g_i + k) % groups
        for i in range(tiles):
            rows = pl.ds(i * q_tile, q_tile)
            arrived(heads.at[src, rows], o_s.at[k, i], o_r.at[src, i], sp=src * ranks + r_i)

    parts = pair_send.shape[1]
    part_cols = width // parts

    def head_rows(chunk):
        start = pl.multiple_of(chunk * own, 16)
        return jnp.concatenate(
            [heads[h, pl.ds(start, own), :] for h in range(groups)], axis=-1
        )

    def term(left, p):
        cols = slice(p * part_cols, (p + 1) * part_cols)
        return jnp.dot(left, wo[:, cols], preferred_element_type=f32).astype(bf16)

    def to_partner(k):
        chip = (chip_i + 1 + k) % chips
        left = head_rows(chip * 2 + (1 - core_i))
        for p in range(parts):
            pair_send[k, p] = term(left, p)
            send(
                pair_send.at[k, p], pair_recv.at[k, p], pair_s.at[k, p], pair_r.at[k, p],
                tp=partner,
            )

    def with_partner(k):
        chip = (chip_i + 1 + k) % chips
        left = head_rows(chip * 2 + core_i)
        for p in range(parts):
            mine = term(left, p).astype(f32)
            arrived(pair_recv.at[k, p], pair_s.at[k, p], pair_r.at[k, p], tp=partner)
            both = mine + pair_recv[k, p].astype(f32)
            if k < chips - 1:
                fin_send[k, p] = both.astype(bf16)
                send(
                    fin_send.at[k, p], fin_recv.at[k, p], fin_s.at[k, p], fin_r.at[k, p],
                    tp=chip * 2 + core_i,
                )
            else:
                own_sum[p] = both

    for k in range(chips - 1):
        to_partner(k)
    for k in range(chips - 1):
        with_partner(k)
    to_partner(chips - 1)
    with_partner(chips - 1)
    for p in range(parts):
        summed = own_sum[p]
        for k in range(chips - 1):
            src_chip = (chip_i + chips - 1 - k) % chips
            arrived(
                fin_recv.at[k, p], fin_s.at[k, p], fin_r.at[k, p], tp=src_chip * 2 + core_i
            )
            summed = summed + fin_recv[k, p].astype(f32)
        cols = slice(p * part_cols, (p + 1) * part_cols)
        per = mod_cols // part_cols
        if per >= 1:
            low = (p % per) * part_cols
            gate = mod_all[p // per, 4:5, low : low + part_cols]
        else:
            span = part_cols // mod_cols
            gate = jnp.concatenate(
                [mod_all[p * span + q, 4:5, :] for q in range(span)], axis=-1
            )
        out[:, cols] = (lat[:, cols].astype(f32) + gate * summed).astype(bf16)
    for copy in pending:
        copy.wait_send()
    for k in order:
        for i in range(tiles):
            o_copy(k, i).wait_send()


def local(
    n_sp,
    n_tp,
    latent,
    context,
    cond_latent,
    cond_context,
    shift_weight,
    scale_weight,
    gate_weight,
    query_weight,
    key_weight,
    value_weight,
    out_weight,
    lambda_heads,
    out_gain,
):
    own, width = latent.shape
    ctx_rows = context.shape[0]
    tok = own * n_tp
    groups = lambda_heads.shape[0]
    ranks = n_sp // groups
    chips = n_tp // 2
    mod_rows, mod_cols = shift_weight.shape
    keys = n_sp * (tok + ctx_rows)
    q_tile = pick(tok, 128, 16)
    pieces = 3 if own % 48 == 0 else 1
    parts = 4 if width % (4 * LANES) == 0 else 1

    quarter = HEAD_DIM // 4
    inverse = np.float32(rope_theta) ** (-np.arange(quarter, dtype=np.float32) / quarter)
    zeros = np.zeros((quarter,), np.float32)
    repeat = LANES // (2 * quarter)
    half = np.ones((2 * quarter,), np.float32)
    lane_table = np.zeros((8, LANES), np.float32)
    lane_table[0] = np.tile(np.concatenate([inverse, zeros]), repeat)
    lane_table[1] = np.tile(np.concatenate([zeros, inverse]), repeat)
    lane_table[2] = np.tile(np.concatenate([-half, half]), repeat // 2)
    gain = out_gain.reshape(groups, 1, VALUE_DIM)
    vmem = pl.BlockSpec(memory_space=pltpu.VMEM)
    hbm = pl.BlockSpec(memory_space=pl.ANY)
    dma = pltpu.SemaphoreType.DMA
    scratch = [
        pltpu.VMEM(query_weight.shape, bf16),
        pltpu.VMEM(key_weight.shape, bf16),
        pltpu.VMEM(value_weight.shape, bf16),
        pltpu.VMEM(out_weight.shape, bf16),
        pltpu.VMEM((8, mod_cols), f32),
        pltpu.VMEM((n_sp, 8, mod_cols), f32),
        pltpu.VMEM((n_tp, 8, mod_cols), f32),
        pltpu.VMEM((n_tp, own, width), bf16),
        pltpu.VMEM((2 * own + ctx_rows, width), bf16),
        pltpu.VMEM((tok, LANES), f32),
        pltpu.VMEM((tok, LANES), f32),
        pltpu.VMEM((groups, tok, LANES), bf16),
        pltpu.VMEM((groups, tok, 2 * LANES), bf16),
        pltpu.VMEM((groups, ctx_rows, 2 * LANES), bf16),
        pltpu.VMEM((groups, tok, LANES), bf16),
        pltpu.VMEM((keys, 2 * LANES), bf16),
        pltpu.VMEM((2 * q_tile, keys), f32),
        pltpu.VMEM((groups, tok, LANES), bf16),
        pltpu.VMEM((groups, tok, LANES), bf16),
        pltpu.VMEM((chips, parts, own, width // parts), bf16),
        pltpu.VMEM((chips, parts, own, width // parts), bf16),
        pltpu.VMEM((max(chips - 1, 1), parts, own, width // parts), bf16),
        pltpu.VMEM((max(chips - 1, 1), parts, own, width // parts), bf16),
        pltpu.VMEM((parts, own, width // parts), f32),
        dma((4,)),
        dma((3,)),
        dma((n_sp,)),
        dma((n_sp,)),
        dma((n_tp,)),
        dma((n_tp,)),
        dma((chips, pieces)),
        dma((chips, pieces)),
        dma((chips, pieces)),
        dma((chips, pieces)),
        dma((groups,)),
        dma((groups,)),
        dma((groups, chips)),
        dma((groups, chips)),
        dma((groups,)),
        dma((groups,)),
        dma((groups, chips, ranks)),
        dma((groups, chips, ranks)),
        dma((groups, ranks)),
        dma((groups, ranks)),
        dma((groups, tok // q_tile)),
        dma((groups, tok // q_tile)),
        dma((chips, parts)),
        dma((chips, parts)),
        dma((chips, parts)),
        dma((chips, parts)),
    ]
    return pl.pallas_call(
        functools.partial(body, n_sp, n_tp),
        out_shape=jax.ShapeDtypeStruct((own, width), bf16),
        in_specs=[vmem] * 8 + [pl.BlockSpec(memory_space=pltpu.SMEM), vmem] + [hbm] * 4,
        out_specs=vmem,
        scratch_shapes=scratch,
        compiler_params=pltpu.CompilerParams(
            collective_id=0, has_side_effects=True, vmem_limit_bytes=60 * 1024 * 1024
        ),
        name="diff_attention",
    )(
        latent,
        context,
        cond_latent.reshape(n_sp, 1, mod_rows),
        cond_context.reshape(n_sp, 1, mod_rows),
        shift_weight,
        scale_weight,
        gate_weight,
        jnp.asarray(lane_table),
        lambda_heads,
        gain,
        query_weight,
        key_weight,
        value_weight,
        out_weight,
    )


def solution(mesh):
    placed = (
        P(("sp", "tp"), None),
        P("sp", None),
        P(),
        P(),
        P("sp", "tp"),
        P("sp", "tp"),
        P("sp", "tp"),
        P(None, None, "tp"),
        P(None, None, "tp"),
        P(None, "tp"),
        P("tp", None),
        P("tp"),
        P("tp"),
    )
    return jax.shard_map(
        functools.partial(local, mesh.shape["sp"], mesh.shape["tp"]),
        mesh=mesh,
        in_specs=placed,
        out_specs=P(("sp", "tp"), None),
        check_vma=False,
    )
```

profile of v0, /device:TPU:0, one launch (start us, length us, event | category | flops | bytes accessed | tf_op | source)
XLA Modules:
  0.0 92.5 jit_solution(17780735585983957353)
XLA Ops:
  0.0 90.7 %diff_attention.1 = bf16[96,2048]{1,0:T(8,128)(2,1)} custom-call(bf16[96,2048]{1,0:T(8,128)(2,1)} %lat.1, bf16[64,2048]{1,0:T(8,128)(2,1)} %ctx.1, f32[8,1,256]{2,1,0:T(1,128)} %bitcast.3, f32[8,1,256]{2,1,0:T(1,128)} %bitcast.4, bf16[256,512]{1,0:T(8,128)(2,1)} %shift_w.1, bf16[256,512]{1,0:T(8,128)(2,1)} %scale_w.1, bf16[256,512]{1,0:T(8,128)(2,1)} %gate_w.1, ...), custom_call_target="tpu_custom_call" | custom-call | tf_op jit(solution)/shard_map/diff_attention/pallas_call | solution.py:624
  90.7 1.8 %copy.16 = bf16[96,2048]{1,0:T(8,128)(2,1)} copy(bf16[96,2048]{1,0:T(8,128)(2,1)} %diff_attention.1) | data formatting | bytes 786432
where the time goes:
time: 92.7 us; the launch traced here: 92.5 us
  Pallas kernels  90.7 us (98%)
  local copies, waits for them, and re-layouts  1.77 us (2%)
    pallas_call x1, Pallas kernels, local(): pl.pallas_call(functools.partial(body, n_sp, n_tp), out_shape=jax.ShapeDt...  90.7 us

commit v1 on v0

--- a/solution.py
+++ b/solution.py
@@ -527,6 +527,683 @@
             o_copy(k, i).wait_send()
 
 
+def split_body(
+    n_sp,
+    n_tp,
+    lat,
+    ctx,
+    cond_l,
+    cond_c,
+    shift_w,
+    scale_w,
+    gate_w,
+    lane_table,
+    lam,
+    gain,
+    wq_hbm,
+    wk_hbm,
+    wv_hbm,
+    wo_hbm,
+    out,
+    w,
+    wo,
+    mod_part,
+    mod_recv,
+    mod_half,
+    mod_far,
+    mod_all,
+    par_own,
+    par_recv,
+    raw,
+    far_ctx,
+    hidden,
+    cos_t,
+    sin_t,
+    kv_send,
+    kvc_send,
+    q_send,
+    kv_buf,
+    q_buf,
+    vals_t,
+    gain_t,
+    peak_s,
+    sum_s,
+    acc_s,
+    o_send,
+    heads,
+    mine,
+    pair_send,
+    pair_recv,
+    fin_send,
+    fin_recv,
+    own_sum,
+    w_sem,
+    par_sem,
+    mod1_s,
+    mod1_r,
+    modf_sem,
+    mod2_s,
+    mod2_r,
+    z_s,
+    z_r,
+    x_s,
+    x_r,
+    d_s,
+    d_r,
+    kv_s,
+    kv_r,
+    kvc_s,
+    kvc_r,
+    q_s,
+    q_r,
+    rel_s,
+    rel_r,
+    relc_s,
+    relc_r,
+    o_s,
+    o_r,
+    pair_s,
+    pair_r,
+    fin_s,
+    fin_r,
+):
+    own, width = lat.shape
+    ctx_rows = ctx.shape[0]
+    tok = own * n_tp
+    mod_cols = shift_w.shape[1]
+    pieces = z_s.shape[0] - 1
+    rows_p = own // pieces
+    ctx_p = ctx_rows // n_tp
+    pair_rows = 2 * rows_p
+    chunk_rows = 2 * pair_rows
+    set_rows = tok + ctx_rows
+    keys = 4 * set_rows
+    q_tile = 4 * pair_rows
+    sp_i = lax.axis_index("sp")
+    tp_i = lax.axis_index("tp")
+    z_i = sp_i // 2
+    y_i = sp_i % 2
+    half_i = z_i // 2
+    zl_i = z_i % 2
+    src_i = zl_i * 2 + y_i
+    x_i = tp_i // 2
+    c_i = tp_i % 2
+    slot_i = c_i * 2 + x_i
+    mirror = (sp_i + 4) % n_sp
+    partner = x_i * 2 + (1 - c_i)
+    across = (1 - x_i) * 2 + c_i
+    owns_head = c_i == y_i
+    pending = []
+    when_remote = []
+
+    def remote(src, dst, s_sem, r_sem, **where):
+        return pltpu.make_async_remote_copy(
+            src_ref=src, dst_ref=dst, send_sem=s_sem, recv_sem=r_sem,
+            device_id=where, device_id_type=MESH,
+        )
+
+    def send(src, dst, s_sem, r_sem, **where):
+        copy = remote(src, dst, s_sem, r_sem, **where)
+        copy.start()
+        pending.append(copy)
+
+    def send_or_keep(src, dst, s_sem, r_sem, **where):
+        copy = remote(src, dst, s_sem, r_sem, **where)
+
+        @pl.when(owns_head)
+        def _():
+            pltpu.make_async_copy(src, dst, r_sem).start()
+
+        @pl.when(jnp.logical_not(owns_head))
+        def _():
+            copy.start()
+
+        when_remote.append(copy)
+
+    def arrived(ref, r_sem):
+        pltpu.make_async_copy(ref, ref, r_sem).wait()
+
+    def sp_at(half, zl, y):
+        return (half * 2 + zl) * 2 + y
+
+    head_cols = 2 * HEAD_DIM
+    val_cols = 2 * VALUE_DIM
+
+    def part_cols_of(start, size):
+        return pl.ds(pl.multiple_of(start, LANES), size)
+
+    loads = []
+    for m in (0, 1):
+        loads.append(
+            (wk_hbm.at[m, :, part_cols_of(half_i * head_cols, head_cols)],
+             w.at[:, pl.ds(m * head_cols, head_cols)])
+        )
+    loads.append(
+        (wv_hbm.at[:, part_cols_of(half_i * val_cols, val_cols)],
+         w.at[:, pl.ds(2 * head_cols, val_cols)])
+    )
+    for m in (0, 1):
+        loads.append(
+            (wq_hbm.at[m, :, part_cols_of(half_i * head_cols, head_cols)],
+             w.at[:, pl.ds(2 * head_cols + val_cols + m * head_cols, head_cols)])
+        )
+    loads.append((wo_hbm, wo))
+    loads = [pltpu.make_async_copy(a, b, w_sem.at[i]) for i, (a, b) in enumerate(loads)]
+    for load in loads:
+        load.start()
+
+    barrier = pltpu.get_barrier_semaphore()
+    for k in range(1, n_sp):
+        for tp in (tp_i, partner):
+            pl.semaphore_signal(
+                barrier, inc=1, device_id={"sp": (sp_i + k) % n_sp, "tp": tp},
+                device_id_type=MESH,
+            )
+    for k in range(1, n_tp):
+        pl.semaphore_signal(
+            barrier, inc=1, device_id={"tp": (tp_i + k) % n_tp}, device_id_type=MESH
+        )
+
+    def silu(v):
+        return (v / (1.0 + jnp.exp(-v))).astype(bf16).astype(f32)
+
+    c0 = silu(cond_l[sp_i])
+    c1 = silu(cond_c[sp_i])
+    row = lax.broadcasted_iota(jnp.int32, (8, c0.shape[-1]), 0)
+
+    def placed_rows(at0, at1):
+        zero = jnp.zeros(row.shape, f32)
+        rows = jnp.where(row == at0, jnp.broadcast_to(c0, row.shape), zero)
+        if at1 is not None:
+            rows = jnp.where(row == at1, jnp.broadcast_to(c1, row.shape), rows)
+        return rows.astype(bf16)
+
+    mod_part[...] = (
+        jnp.dot(placed_rows(0, 1), shift_w[...], preferred_element_type=f32)
+        + jnp.dot(placed_rows(2, 3), scale_w[...], preferred_element_type=f32)
+        + jnp.dot(placed_rows(4, None), gate_w[...], preferred_element_type=f32)
+    )
+    par_own[0:1, :] = gain[z_i]
+    par_own[1:2, :] = jnp.full((1, VALUE_DIM), lam[z_i], f32)
+    pl.semaphore_wait(barrier, 2 * (n_sp - 1) + n_tp - 1)
+
+    mates = [(dz, dy) for dz in (0, 1) for dy in (0, 1) if dz or dy]
+    for e, (dz, dy) in enumerate(mates):
+        send(
+            mod_part, mod_recv.at[src_i], mod1_s.at[e], mod1_r.at[src_i],
+            sp=sp_at(half_i, (zl_i + dz) % 2, (y_i + dy) % 2),
+        )
+
+    def piece(s, slot, p):
+        if p == pieces:
+            return far_ctx.at[pl.ds(slot * ctx_p, ctx_p)]
+        return raw.at[s, slot, pl.ds(p * rows_p, rows_p)]
+
+    def send_far(p):
+        src = (
+            ctx.at[pl.ds(pl.multiple_of(tp_i * ctx_p, ctx_p), ctx_p)]
+            if p == pieces
+            else lat.at[pl.ds(p * rows_p, rows_p)]
+        )
+        send(src, piece(1, slot_i, p), z_s.at[p], z_r.at[p], sp=mirror)
+
+    def spread_x(s, p):
+        src = piece(s, slot_i, p)
+        if s == 0:
+            src = lat.at[pl.ds(p * rows_p, rows_p)]
+        send(src, piece(s, slot_i, p), x_s.at[s, p], x_r.at[s, p], tp=across)
+
+    def spread_d(s, p):
+        src = piece(s, slot_i, p)
+        if s == 0:
+            src = lat.at[pl.ds(p * rows_p, rows_p)]
+        send(src, piece(s, slot_i, p), d_s.at[s, p, 0], d_r.at[s, p, 0], tp=partner)
+
+    def from_far(p):
+        arrived(piece(1, slot_i, p), z_r.at[p])
+        spread_x(1, p)
+        spread_d(1, p)
+
+    def from_across(s, p):
+        slot = c_i * 2 + (1 - x_i)
+        arrived(piece(s, slot, p), x_r.at[s, p])
+        send(piece(s, slot, p), piece(s, slot, p), d_s.at[s, p, 1], d_r.at[s, p, 1], tp=partner)
+
+    def from_partner(s, p):
+        arrived(piece(s, (1 - c_i) * 2 + x_i, p), d_r.at[s, p, 0])
+        arrived(piece(s, (1 - c_i) * 2 + (1 - x_i), p), d_r.at[s, p, 1])
+
+    send_far(pieces)
+    for p in range(pieces):
+        spread_d(0, p)
+    for p in range(pieces - 1):
+        spread_x(0, p)
+    send(par_own, par_recv, par_sem.at[0], par_sem.at[1], tp=partner)
+    raw[0, slot_i] = lat[...]
+    mod_recv[src_i] = mod_part[...]
+
+    def fill_rope(s):
+        place = lax.broadcasted_iota(jnp.int32, (chunk_rows, LANES), 0)
+        core = place // pair_rows
+        chip = (place // rows_p) % 2
+        home = sp_i if s == 0 else mirror
+        for p in range(pieces):
+            tok_row = home * tok + (chip * 2 + core) * own + p * rows_p + place % rows_p
+            grid_row = (tok_row // GRID_W).astype(f32)
+            grid_col = (tok_row % GRID_W).astype(f32)
+            angles = grid_row * lane_table[0:1, :] + grid_col * lane_table[1:2, :]
+            cos_t[s, p] = jnp.cos(angles)
+            sin_t[s, p] = jnp.sin(angles) * lane_table[2:3, :]
+
+    fill_rope(0)
+
+    for dz, dy in mates:
+        src = (zl_i + dz) % 2 * 2 + (y_i + dy) % 2
+        arrived(mod_recv.at[src], mod1_r.at[src])
+    total = mod_recv[0]
+    for k in range(1, 4):
+        total = total + mod_recv[k]
+    mod_half[...] = total
+    send(mod_half, mod_far, modf_sem.at[0], modf_sem.at[1], sp=mirror)
+    for p in range(pieces):
+        send_far(p)
+
+    fill_rope(1)
+
+    arrived(mod_far, modf_sem.at[1])
+    mod_all[tp_i] = total + mod_far[...]
+    for k in range(1, n_tp):
+        send(
+            mod_all.at[tp_i], mod_all.at[tp_i], mod2_s.at[k], mod2_r.at[tp_i],
+            tp=(tp_i + k) % n_tp,
+        )
+    spread_x(0, pieces - 1)
+    from_far(pieces)
+    for p in range(pieces - 1):
+        from_across(0, p)
+    for k in range(1, n_tp):
+        src = (tp_i + n_tp - k) % n_tp
+        arrived(mod_all.at[src], mod2_r.at[src])
+
+    def modulate(x, which, start):
+        at = pl.ds(start, x.shape[0])
+        factor = lax.rsqrt(jnp.mean(x * x, axis=-1, keepdims=True) + norm_eps)
+        for t in range(n_tp):
+            cols = slice(t * mod_cols, (t + 1) * mod_cols)
+            shift = mod_all[t, which : which + 1, :]
+            scale = mod_all[t, which + 2 : which + 3, :]
+            hidden[at, cols] = (
+                (x[:, cols] * factor) * (1.0 + scale) + shift
+            ).astype(bf16)
+
+    lane = lax.broadcasted_iota(jnp.int32, (chunk_rows, LANES), 1)
+    first_quarter = lane % HEAD_DIM < HEAD_DIM // 2
+    low_half = lane < HEAD_DIM
+    ctx_half = lax.broadcasted_iota(jnp.int32, (ctx_rows, LANES), 1) < HEAD_DIM
+
+    def rope(u, s, p):
+        swapped = jnp.where(
+            first_quarter,
+            pltpu.roll(u, LANES - HEAD_DIM // 2, 1),
+            pltpu.roll(u, HEAD_DIM // 2, 1),
+        )
+        return u * cos_t[s, p] + swapped * sin_t[s, p]
+
+    def pair_up(a, b, low):
+        return (
+            jnp.where(low, a, pltpu.roll(b, HEAD_DIM, 1)).astype(bf16),
+            jnp.where(low, pltpu.roll(a, HEAD_DIM, 1), b).astype(bf16),
+        )
+
+    def kv_at(s, src, core, p):
+        start = (s * 4 + src) * set_rows + core * (tok // 2) + p * pair_rows
+        return kv_buf.at[pl.ds(pl.multiple_of(start, 16), pair_rows)]
+
+    def kvc_at(s, src, core):
+        start = (s * 4 + src) * set_rows + tok + core * (ctx_rows // 2)
+        return kv_buf.at[pl.ds(pl.multiple_of(start, 16), ctx_rows // 2)]
+
+    def q_at(s, src, p):
+        start = ((s * pieces + p) * 4 + src) * pair_rows
+        return pl.ds(pl.multiple_of(start, 16), pair_rows)
+
+    def chunk(s, p, with_ctx):
+        from_partner(s, p)
+        for slot in range(4):
+            modulate(
+                raw[s, slot, p * rows_p : (p + 1) * rows_p, :].astype(f32), 0, slot * rows_p
+            )
+        count = chunk_rows
+        if with_ctx:
+            if s == 1:
+                from_partner(1, pieces)
+                modulate(far_ctx[...].astype(f32), 1, chunk_rows)
+            else:
+                modulate(ctx[...].astype(f32), 1, chunk_rows)
+            count = chunk_rows + ctx_rows
+        if s == 0 and p == 0:
+            for load in loads[:5]:
+                load.wait()
+        kv_cols = 2 * head_cols + val_cols
+        kv = jnp.dot(hidden[:count, :], w[:, :kv_cols], preferred_element_type=f32)
+        slabs = [kv[:, m * LANES : (m + 1) * LANES] for m in (0, 1)]
+        pair = pair_up(
+            rope(slabs[0][:chunk_rows], s, p), rope(slabs[1][:chunk_rows], s, p), low_half
+        )
+        if with_ctx:
+            pair_c = pair_up(slabs[0][chunk_rows:], slabs[1][chunk_rows:], ctx_half)
+        for j in (0, 1):
+            vals = kv[:, (2 + j) * LANES : (3 + j) * LANES].astype(bf16)
+            for core in (0, 1):
+                rows = slice(core * pair_rows, (core + 1) * pair_rows)
+                kv_send[s, j, core, p, :, :LANES] = pair[j][rows]
+                kv_send[s, j, core, p, :, LANES:] = vals[rows]
+            if with_ctx:
+                kvc_send[s, j, :, :LANES] = pair_c[j]
+                kvc_send[s, j, :, LANES:] = vals[chunk_rows:]
+        for dj in (1, 0):
+            j = (zl_i + dj) % 2
+            for dc in (0, 1):
+                core = (c_i + dc) % 2
+                put = send if dj or dc else send_or_keep
+                where = dict(sp=sp_at(half_i, j, c_i), tp=x_i * 2 + core)
+                put(
+                    kv_send.at[s, j, core, p], kv_at(s, src_i, core, p),
+                    kv_s.at[s, p, dj, dc], kv_r.at[s, src_i, p], **where,
+                )
+                if with_ctx:
+                    half = pl.ds(pl.multiple_of(core * (ctx_rows // 2), 16), ctx_rows // 2)
+                    put(
+                        kvc_send.at[s, j, half], kvc_at(s, src_i, core),
+                        kvc_s.at[s, dj, dc], kvc_r.at[s, src_i], **where,
+                    )
+        q = jnp.dot(hidden[:chunk_rows, :], w[:, kv_cols:], preferred_element_type=f32)
+        pair = pair_up(rope(q[:, :LANES], s, p), rope(q[:, LANES:], s, p), low_half)
+        for j in (0, 1):
+            for core in (0, 1):
+                q_send[s, j, core, p] = pair[j][core * pair_rows : (core + 1) * pair_rows]
+        for dj in (1, 0):
+            j = (zl_i + dj) % 2
+            for dc in (0, 1):
+                core = (c_i + dc) % 2
+                put = send if dj or dc else send_or_keep
+                put(
+                    q_send.at[s, j, core, p], q_buf.at[q_at(s, src_i, p)],
+                    q_s.at[s, p, dj, dc], q_r.at[s, src_i, p],
+                    sp=sp_at(half_i, j, c_i), tp=x_i * 2 + core,
+                )
+
+    def relay(s, p, with_ctx):
+        for src in range(4):
+            arrived(kv_at(s, src, c_i, p), kv_r.at[s, src, p])
+            send(
+                kv_at(s, src, c_i, p), kv_at(s, src, c_i, p),
+                rel_s.at[s, src, p], rel_r.at[s, src, p], tp=partner,
+            )
+            if with_ctx:
+                arrived(kvc_at(s, src, c_i), kvc_r.at[s, src])
+                send(
+                    kvc_at(s, src, c_i), kvc_at(s, src, c_i),
+                    relc_s.at[s, src], relc_r.at[s, src], tp=partner,
+                )
+
+    def wait_keys(s):
+        for src in range(4):
+            for p in range(pieces):
+                arrived(kv_at(s, src, 1 - c_i, p), rel_r.at[s, src, p])
+            arrived(kvc_at(s, src, 1 - c_i), relc_r.at[s, src])
+        step = 2 * LANES
+        for b in range(keys // step):
+            at = s * keys + b * step
+            vals_t[s, :, b * step : (b + 1) * step] = kv_buf[at : at + step, LANES:].T
+
+    def wait_queries(s, p):
+        for src in range(4):
+            arrived(q_buf.at[q_at(s, src, p)], q_r.at[s, src, p])
+
+    coef = HEAD_DIM ** (-0.5) * 1.4426950408889634
+    q_low = lax.broadcasted_iota(jnp.int32, (q_tile, LANES), 1) < HEAD_DIM
+    cols = 2 * q_tile
+
+    def item(tile, s, first, last):
+        q = q_buf[tile * q_tile : (tile + 1) * q_tile, :]
+        zero = jnp.zeros_like(q)
+        q2 = jnp.concatenate([jnp.where(q_low, q, zero), jnp.where(q_low, zero, q)], axis=0)
+        scores = lax.dot_general(
+            kv_buf[s * keys : (s + 1) * keys, :LANES], q2, (((1,), (1,)), ((), ())),
+            preferred_element_type=f32,
+        )
+        peak = jnp.max(scores, axis=0, keepdims=True)
+        if not first:
+            old = peak_s[tile]
+            peak = jnp.maximum(old, peak)
+        weights = jnp.exp2(scores * coef - peak * coef)
+        sums = jnp.sum(weights.reshape(keys // 8, 8, cols), axis=0)
+        acc = jnp.dot(vals_t[s], weights.astype(bf16), preferred_element_type=f32)
+        if not first:
+            fade = jnp.exp2((old - peak) * coef)
+            sums = sums + sum_s[tile] * fade
+            acc = acc + acc_s[tile] * fade
+        if not last:
+            peak_s[tile] = peak
+            sum_s[tile] = sums
+            acc_s[tile] = acc
+            return
+        mean_v = acc / jnp.sum(sums, axis=0, keepdims=True)
+        mixed = mean_v[:, :q_tile] - gain_t[VALUE_DIM : VALUE_DIM + 1, :] * mean_v[:, q_tile:]
+        factor = lax.rsqrt(jnp.mean(mixed * mixed, axis=0, keepdims=True) + norm_eps)
+        o_send[tile * q_tile : (tile + 1) * q_tile, :] = (
+            mixed * factor * gain_t[:VALUE_DIM, :]
+        ).T.astype(bf16)
+
+    def give_back(s, p):
+        half = half_i if s == 0 else 1 - half_i
+        for dz, dy in mates + [(0, 0)]:
+            zl = (zl_i + dz) % 2
+            y = (y_i + dy) % 2
+            put = send if s or dz or dy else send_or_keep
+            put(
+                o_send.at[q_at(s, zl * 2 + y, p)], heads.at[z_i, c_i, p],
+                o_s.at[s, p, dz * 2 + dy], o_r.at[z_i, c_i, p],
+                sp=sp_at(half, zl, y), tp=x_i * 2 + y_i,
+            )
+
+    parts = pair_send.shape[1]
+    part_cols = width // parts
+
+    def project(p):
+        for h in range(4):
+            for core in (0, 1):
+                arrived(heads.at[h, core, p], o_r.at[h, core, p])
+        left = jnp.concatenate(
+            [
+                jnp.concatenate([heads[h, core, p] for h in range(4)], axis=-1)
+                for core in (1 - c_i, c_i)
+            ],
+            axis=0,
+        )
+        for k in range(parts):
+            at = slice(k * part_cols, (k + 1) * part_cols)
+            terms = jnp.dot(left, wo[:, at], preferred_element_type=f32).astype(bf16)
+            pair_send[p, k] = terms[:pair_rows]
+            mine[p, k] = terms[pair_rows:]
+            send(
+                pair_send.at[p, k], pair_recv.at[p, k], pair_s.at[p, k], pair_r.at[p, k],
+                tp=partner,
+            )
+
+    def combine(p):
+        here = pl.ds(pl.multiple_of(x_i * rows_p, rows_p), rows_p)
+        there = pl.ds(pl.multiple_of((1 - x_i) * rows_p, rows_p), rows_p)
+        for k in range(parts):
+            arrived(pair_recv.at[p, k], pair_r.at[p, k])
+            both = mine[p, k, there, :].astype(f32) + pair_recv[p, k, there, :].astype(f32)
+            fin_send[p, k] = both.astype(bf16)
+            send(
+                fin_send.at[p, k], fin_recv.at[p, k], fin_s.at[p, k], fin_r.at[p, k], tp=across
+            )
+            own_sum[p, k] = mine[p, k, here, :].astype(f32) + pair_recv[p, k, here, :].astype(f32)
+
+    def finish(p):
+        rows = slice(p * rows_p, (p + 1) * rows_p)
+        for k in range(parts):
+            arrived(fin_recv.at[p, k], fin_r.at[p, k])
+            summed = own_sum[p, k] + fin_recv[p, k].astype(f32)
+            done = 0
+            while done < part_cols:
+                col = k * part_cols + done
+                size = min(mod_cols - col % mod_cols, part_cols - done)
+                at = slice(col, col + size)
+                low = col % mod_cols
+                gate = mod_all[col // mod_cols, 4:5, low : low + size]
+                out[rows, at] = (
+                    lat[rows, at].astype(f32) + gate * summed[:, done : done + size]
+                ).astype(bf16)
+                done += size
+
+    last = pieces - 1
+    for p in range(last):
+        chunk(0, p, p == 0)
+        if p == 0:
+            from_across(1, pieces)
+    from_far(0)
+    from_across(0, last)
+    chunk(0, last, False)
+    arrived(par_recv, par_sem.at[1])
+    params = jnp.where(owns_head, par_own[...], par_recv[...])
+    gain_row = jnp.broadcast_to(params[0:1, :], (VALUE_DIM, VALUE_DIM)).T
+    lam_row = jnp.broadcast_to(params[1:2, :], (8, VALUE_DIM))
+    for k in range(q_tile // VALUE_DIM):
+        gain_t[:VALUE_DIM, k * VALUE_DIM : (k + 1) * VALUE_DIM] = gain_row
+        gain_t[VALUE_DIM:, k * VALUE_DIM : (k + 1) * VALUE_DIM] = lam_row
+    from_across(1, 0)
+    chunk(1, 0, True)
+    for p in range(last):
+        relay(0, p, p == 0)
+    for p in range(1, last):
+        from_far(p)
+        from_across(1, p)
+        chunk(1, p, False)
+    relay(0, last, False)
+    wait_keys(0)
+    for p in range(pieces):
+        wait_queries(0, p)
+    item(0, 0, True, False)
+    from_far(last)
+    item(1, 0, True, False)
+    from_across(1, last)
+    chunk(1, last, False)
+    item(2, 0, True, False)
+    for p in range(last):
+        relay(1, p, p == 0)
+    for p in range(last):
+        wait_queries(1, p)
+        item(pieces + p, 0, True, False)
+    relay(1, last, False)
+    wait_keys(1)
+    wait_queries(1, last)
+    for p in range(pieces):
+        if p == last:
+            item(pieces + p, 0, True, False)
+        item(pieces + p, 1, False, True)
+        give_back(1, p)
+        if p > 0:
+            project(p - 1)
+        item(p, 1, False, True)
+        give_back(0, p)
+        if p == 0:
+            loads[5].wait()
+        else:
+            combine(p - 1)
+    project(last)
+    for p in range(last):
+        finish(p)
+    combine(last)
+    finish(last)
+    for copy in pending:
+        copy.wait_send()
+
+    @pl.when(jnp.logical_not(owns_head))
+    def _():
+        for copy in when_remote:
+            copy.wait_send()
+
+
+def split_scratch(n_sp, n_tp, own, width, ctx_rows, mod_cols, groups):
+    tok = own * n_tp
+    pieces = 3
+    rows_p = own // pieces
+    pair_rows = 2 * rows_p
+    q_tile = 4 * pair_rows
+    keys = 4 * (tok + ctx_rows)
+    parts = 2
+    part_cols = width // parts
+    dma = pltpu.SemaphoreType.DMA
+    return [
+        pltpu.VMEM((width, 4 * 2 * HEAD_DIM + 2 * VALUE_DIM), bf16),
+        pltpu.VMEM((groups * VALUE_DIM, width), bf16),
+        pltpu.VMEM((8, mod_cols), f32),
+        pltpu.VMEM((4, 8, mod_cols), f32),
+        pltpu.VMEM((8, mod_cols), f32),
+        pltpu.VMEM((8, mod_cols), f32),
+        pltpu.VMEM((n_tp, 8, mod_cols), f32),
+        pltpu.VMEM((8, VALUE_DIM), f32),
+        pltpu.VMEM((8, VALUE_DIM), f32),
+        pltpu.VMEM((2, 4, own, width), bf16),
+        pltpu.VMEM((ctx_rows, width), bf16),
+        pltpu.VMEM((2 * pair_rows + ctx_rows, width), bf16),
+        pltpu.VMEM((2, pieces, 2 * pair_rows, LANES), f32),
+        pltpu.VMEM((2, pieces, 2 * pair_rows, LANES), f32),
+        pltpu.VMEM((2, 2, 2, pieces, pair_rows, 2 * LANES), bf16),
+        pltpu.VMEM((2, 2, ctx_rows, 2 * LANES), bf16),
+        pltpu.VMEM((2, 2, 2, pieces, pair_rows, LANES), bf16),
+        pltpu.VMEM((2 * keys, 2 * LANES), bf16),
+        pltpu.VMEM((2 * pieces * q_tile, LANES), bf16),
+        pltpu.VMEM((2, VALUE_DIM, keys), bf16),
+        pltpu.VMEM((VALUE_DIM + 8, q_tile), f32),
+        pltpu.VMEM((2 * pieces, 1, 2 * q_tile), f32),
+        pltpu.VMEM((2 * pieces, 8, 2 * q_tile), f32),
+        pltpu.VMEM((2 * pieces, VALUE_DIM, 2 * q_tile), f32),
+        pltpu.VMEM((2 * pieces * q_tile, LANES), bf16),
+        pltpu.VMEM((4, 2, pieces, pair_rows, LANES), bf16),
+        pltpu.VMEM((pieces, parts, pair_rows, part_cols), bf16),
+        pltpu.VMEM((pieces, parts, pair_rows, part_cols), bf16),
+        pltpu.VMEM((pieces, parts, pair_rows, part_cols), bf16),
+        pltpu.VMEM((pieces, parts, rows_p, part_cols), bf16),
+        pltpu.VMEM((pieces, parts, rows_p, part_cols), bf16),
+        pltpu.VMEM((pieces, parts, rows_p, part_cols), f32),
+        dma((6,)),
+        dma((2,)),
+        dma((3,)),
+        dma((4,)),
+        dma((2,)),
+        dma((n_tp,)),
+        dma((n_tp,)),
+        dma((pieces + 1,)),
+        dma((pieces + 1,)),
+        dma((2, pieces + 1)),
+        dma((2, pieces + 1)),
+        dma((2, pieces + 1, 2)),
+        dma((2, pieces + 1, 2)),
+        dma((2, pieces, 2, 2)),
+        dma((2, 4, pieces)),
+        dma((2, 2, 2)),
+        dma((2, 4)),
+        dma((2, pieces, 2, 2)),
+        dma((2, 4, pieces)),
+        dma((2, 4, pieces)),
+        dma((2, 4, pieces)),
+        dma((2, 4)),
+        dma((2, 4)),
+        dma((2, pieces, 4)),
+        dma((4, 2, pieces)),
+        dma((pieces, parts)),
+        dma((pieces, parts)),
+        dma((pieces, parts)),
+        dma((pieces, parts)),
+    ]
+
+
 def local(
     n_sp,
     n_tp,
@@ -621,8 +1298,13 @@
         dma((chips, parts)),
         dma((chips, parts)),
     ]
+    kernel = body
+    fits = own % 48 == 0 and ctx_rows % (16 * n_tp) == 0 and own * 8 // 3 % LANES == 0
+    if (n_sp, n_tp, groups) == (8, 4, 4) and fits and (tok + ctx_rows) % 64 == 0:
+        kernel = split_body
+        scratch = split_scratch(n_sp, n_tp, own, width, ctx_rows, mod_cols, groups)
     return pl.pallas_call(
-        functools.partial(body, n_sp, n_tp),
+        functools.partial(kernel, n_sp, n_tp),
         out_shape=jax.ShapeDtypeStruct((own, width), bf16),
         in_specs=[vmem] * 8 + [pl.BlockSpec(memory_space=pltpu.SMEM), vmem] + [hbm] * 4,
         out_specs=vmem,

time: 92.7 us -> 90.1 us (0.972)
  Pallas kernels: 90.7 us -> 88.1 us
    pallas_call x1, Pallas kernels: 90.7 us -> 88.1 us  [local(): pl.pallas_call(functools.partial(kernel, n_sp, n_tp), out_shape=jax.Shape...]
where the time goes in v1:
time: 90.1 us; the launch traced here: 89.9 us
  Pallas kernels  88.1 us (98%)
  local copies, waits for them, and re-layouts  1.77 us (2%)
    pallas_call x1, Pallas kernels, local(): pl.pallas_call(functools.partial(kernel, n_sp, n_tp), out_shape=jax.Shape...  88.1 us

profile of v1, /device:TPU:0, one launch (start us, length us, event | category | flops | bytes accessed | tf_op | source)
XLA Modules:
  0.0 89.9 jit_solution(10985117938290703097)
XLA Ops:
  0.0 88.1 %diff_attention.1 = bf16[96,2048]{1,0:T(8,128)(2,1)} custom-call(bf16[96,2048]{1,0:T(8,128)(2,1)} %lat.1, bf16[64,2048]{1,0:T(8,128)(2,1)} %ctx.1, f32[8,1,256]{2,1,0:T(1,128)} %bitcast.3, f32[8,1,256]{2,1,0:T(1,128)} %bitcast.4, bf16[256,512]{1,0:T(8,128)(2,1)} %shift_w.1, bf16[256,512]{1,0:T(8,128)(2,1)} %scale_w.1, bf16[256,512]{1,0:T(8,128)(2,1)} %gate_w.1, ...), custom_call_target="tpu_custom_call" | custom-call | tf_op jit(solution)/shard_map/diff_attention/pallas_call | solution.py:1306
  88.1 1.8 %copy.16 = bf16[96,2048]{1,0:T(8,128)(2,1)} copy(bf16[96,2048]{1,0:T(8,128)(2,1)} %diff_attention.1) | data formatting | bytes 786432

commit v2 on v1

--- a/solution.py
+++ b/solution.py
@@ -549,9 +549,10 @@
     wo,
     mod_part,
     mod_recv,
-    mod_half,
-    mod_far,
     mod_all,
+    gate_part,
+    gate_recv,
+    gate_all,
     par_own,
     par_recv,
     raw,
@@ -579,27 +580,17 @@
     own_sum,
     w_sem,
     par_sem,
-    mod1_s,
-    mod1_r,
-    modf_sem,
-    mod2_s,
-    mod2_r,
-    z_s,
+    mod_sem,
+    gate_sem,
+    raw_s,
     z_r,
-    x_s,
     x_r,
-    d_s,
     d_r,
     kv_s,
     kv_r,
-    kvc_s,
-    kvc_r,
+    rel_r,
     q_s,
     q_r,
-    rel_s,
-    rel_r,
-    relc_s,
-    relc_r,
     o_s,
     o_r,
     pair_s,
@@ -611,7 +602,7 @@
     ctx_rows = ctx.shape[0]
     tok = own * n_tp
     mod_cols = shift_w.shape[1]
-    pieces = z_s.shape[0] - 1
+    pieces = z_r.shape[0] - 1
     rows_p = own // pieces
     ctx_p = ctx_rows // n_tp
     pair_rows = 2 * rows_p
@@ -633,8 +624,6 @@
     partner = x_i * 2 + (1 - c_i)
     across = (1 - x_i) * 2 + c_i
     owns_head = c_i == y_i
-    pending = []
-    when_remote = []
 
     def remote(src, dst, s_sem, r_sem, **where):
         return pltpu.make_async_remote_copy(
@@ -643,9 +632,7 @@
         )
 
     def send(src, dst, s_sem, r_sem, **where):
-        copy = remote(src, dst, s_sem, r_sem, **where)
-        copy.start()
-        pending.append(copy)
+        remote(src, dst, s_sem, r_sem, **where).start()
 
     def send_or_keep(src, dst, s_sem, r_sem, **where):
         copy = remote(src, dst, s_sem, r_sem, **where)
@@ -657,8 +644,6 @@
         @pl.when(jnp.logical_not(owns_head))
         def _():
             copy.start()
-
-        when_remote.append(copy)
 
     def arrived(ref, r_sem):
         pltpu.make_async_copy(ref, ref, r_sem).wait()
@@ -687,8 +672,8 @@
             (wq_hbm.at[m, :, part_cols_of(half_i * head_cols, head_cols)],
              w.at[:, pl.ds(2 * head_cols + val_cols + m * head_cols, head_cols)])
         )
-    loads.append((wo_hbm, wo))
-    loads = [pltpu.make_async_copy(a, b, w_sem.at[i]) for i, (a, b) in enumerate(loads)]
+    loads = [pltpu.make_async_copy(a, b, w_sem.at[0]) for a, b in loads]
+    loads.append(pltpu.make_async_copy(wo_hbm, wo, w_sem.at[1]))
     for load in loads:
         load.start()
 
@@ -718,26 +703,49 @@
             rows = jnp.where(row == at1, jnp.broadcast_to(c1, row.shape), rows)
         return rows.astype(bf16)
 
-    mod_part[...] = (
-        jnp.dot(placed_rows(0, 1), shift_w[...], preferred_element_type=f32)
-        + jnp.dot(placed_rows(2, 3), scale_w[...], preferred_element_type=f32)
-        + jnp.dot(placed_rows(4, None), gate_w[...], preferred_element_type=f32)
-    )
+    half_cols = mod_cols // 2
+    mod_total = None
+    for k in (0, 1):
+        at = slice(k * half_cols, (k + 1) * half_cols)
+        for first, weight in ((4 * k, shift_w), (4 * k + 2, scale_w)):
+            term = jnp.dot(
+                placed_rows(first, first + 1), weight[:, at], preferred_element_type=f32
+            )
+            mod_total = term if mod_total is None else mod_total + term
+    mod_part[...] = mod_total
     par_own[0:1, :] = gain[z_i]
     par_own[1:2, :] = jnp.full((1, VALUE_DIM), lam[z_i], f32)
     pl.semaphore_wait(barrier, 2 * (n_sp - 1) + n_tp - 1)
 
-    mates = [(dz, dy) for dz in (0, 1) for dy in (0, 1) if dz or dy]
-    for e, (dz, dy) in enumerate(mates):
-        send(
-            mod_part, mod_recv.at[src_i], mod1_s.at[e], mod1_r.at[src_i],
-            sp=sp_at(half_i, (zl_i + dz) % 2, (y_i + dy) % 2),
-        )
+    def to_all_sp(src, dst, sems):
+        for k in range(1, n_sp):
+            send(src, dst.at[sp_i], sems.at[0], sems.at[1], sp=(sp_i + k) % n_sp)
+
+    def to_all_tp(ref, sems):
+        for k in range(1, n_tp):
+            send(ref.at[tp_i], ref.at[tp_i], sems.at[2], sems.at[3], tp=(tp_i + k) % n_tp)
+
+    def sum_sp(ref, sems):
+        arrived(ref.at[pl.ds(0, n_sp - 1)], sems.at[1])
+        total = ref[0]
+        for k in range(1, n_sp):
+            total = total + ref[k]
+        return total
+
+    mates = [(0, 1), (1, 0), (1, 1)]
+    to_all_sp(mod_part, mod_recv, mod_sem)
 
     def piece(s, slot, p):
         if p == pieces:
-            return far_ctx.at[pl.ds(slot * ctx_p, ctx_p)]
-        return raw.at[s, slot, pl.ds(p * rows_p, rows_p)]
+            return far_ctx.at[pl.ds(pl.multiple_of(slot * ctx_p, 16), ctx_p)]
+        start = ((s * pieces + p) * 4 + slot) * rows_p
+        return raw.at[pl.ds(pl.multiple_of(start, 16), rows_p)]
+
+    def piece_pair(s, core, p):
+        if p == pieces:
+            return far_ctx.at[pl.ds(pl.multiple_of(core * 2 * ctx_p, 16), 2 * ctx_p)]
+        start = ((s * pieces + p) * 4 + core * 2) * rows_p
+        return raw.at[pl.ds(pl.multiple_of(start, 16), pair_rows)]
 
     def send_far(p):
         src = (
@@ -745,19 +753,19 @@
             if p == pieces
             else lat.at[pl.ds(p * rows_p, rows_p)]
         )
-        send(src, piece(1, slot_i, p), z_s.at[p], z_r.at[p], sp=mirror)
+        send(src, piece(1, slot_i, p), raw_s.at[0], z_r.at[p], sp=mirror)
 
     def spread_x(s, p):
         src = piece(s, slot_i, p)
         if s == 0:
             src = lat.at[pl.ds(p * rows_p, rows_p)]
-        send(src, piece(s, slot_i, p), x_s.at[s, p], x_r.at[s, p], tp=across)
+        send(src, piece(s, slot_i, p), raw_s.at[0], x_r.at[s, p], tp=across)
 
     def spread_d(s, p):
         src = piece(s, slot_i, p)
         if s == 0:
             src = lat.at[pl.ds(p * rows_p, rows_p)]
-        send(src, piece(s, slot_i, p), d_s.at[s, p, 0], d_r.at[s, p, 0], tp=partner)
+        send(src, piece(s, slot_i, p), raw_s.at[0], d_r.at[s, p], tp=partner)
 
     def from_far(p):
         arrived(piece(1, slot_i, p), z_r.at[p])
@@ -767,20 +775,18 @@
     def from_across(s, p):
         slot = c_i * 2 + (1 - x_i)
         arrived(piece(s, slot, p), x_r.at[s, p])
-        send(piece(s, slot, p), piece(s, slot, p), d_s.at[s, p, 1], d_r.at[s, p, 1], tp=partner)
+        send(piece(s, slot, p), piece(s, slot, p), raw_s.at[0], d_r.at[s, p], tp=partner)
 
     def from_partner(s, p):
-        arrived(piece(s, (1 - c_i) * 2 + x_i, p), d_r.at[s, p, 0])
-        arrived(piece(s, (1 - c_i) * 2 + (1 - x_i), p), d_r.at[s, p, 1])
-
-    send_far(pieces)
+        arrived(piece_pair(s, 1 - c_i, p), d_r.at[s, p])
+
+    spread_x(0, 0)
     for p in range(pieces):
         spread_d(0, p)
-    for p in range(pieces - 1):
-        spread_x(0, p)
     send(par_own, par_recv, par_sem.at[0], par_sem.at[1], tp=partner)
-    raw[0, slot_i] = lat[...]
-    mod_recv[src_i] = mod_part[...]
+    for p in range(pieces):
+        piece(0, slot_i, p)[...] = lat[p * rows_p : (p + 1) * rows_p, :]
+    mod_recv[sp_i] = mod_part[...]
 
     def fill_rope(s):
         place = lax.broadcasted_iota(jnp.int32, (chunk_rows, LANES), 0)
@@ -796,45 +802,46 @@
             sin_t[s, p] = jnp.sin(angles) * lane_table[2:3, :]
 
     fill_rope(0)
-
-    for dz, dy in mates:
-        src = (zl_i + dz) % 2 * 2 + (y_i + dy) % 2
-        arrived(mod_recv.at[src], mod1_r.at[src])
-    total = mod_recv[0]
-    for k in range(1, 4):
-        total = total + mod_recv[k]
-    mod_half[...] = total
-    send(mod_half, mod_far, modf_sem.at[0], modf_sem.at[1], sp=mirror)
-    for p in range(pieces):
-        send_far(p)
-
     fill_rope(1)
-
-    arrived(mod_far, modf_sem.at[1])
-    mod_all[tp_i] = total + mod_far[...]
-    for k in range(1, n_tp):
-        send(
-            mod_all.at[tp_i], mod_all.at[tp_i], mod2_s.at[k], mod2_r.at[tp_i],
-            tp=(tp_i + k) % n_tp,
-        )
-    spread_x(0, pieces - 1)
-    from_far(pieces)
-    for p in range(pieces - 1):
-        from_across(0, p)
-    for k in range(1, n_tp):
-        src = (tp_i + n_tp - k) % n_tp
-        arrived(mod_all.at[src], mod2_r.at[src])
+    gate_total = None
+    gate_cols = mod_cols // 4
+    for k in range(4):
+        term = jnp.dot(
+            placed_rows(k, None), gate_w[:, k * gate_cols : (k + 1) * gate_cols],
+            preferred_element_type=f32,
+        )
+        gate_total = term if gate_total is None else gate_total + term
+    gate_part[...] = gate_total
+    gate_recv[sp_i] = gate_total
+
+    mod_all[tp_i] = sum_sp(mod_recv, mod_sem)
+    to_all_tp(mod_all, mod_sem)
+    outer = zl_i != half_i
+
+    @pl.when(outer)
+    def _():
+        send_far(pieces)
+        for p in range(pieces):
+            send_far(p)
+
+    for p in range(1, pieces):
+        spread_x(0, p)
+    to_all_sp(gate_part, gate_recv, gate_sem)
+    from_across(0, 0)
+    arrived(mod_all.at[pl.ds(0, n_tp - 1)], mod_sem.at[3])
 
     def modulate(x, which, start):
         at = pl.ds(start, x.shape[0])
         factor = lax.rsqrt(jnp.mean(x * x, axis=-1, keepdims=True) + norm_eps)
         for t in range(n_tp):
-            cols = slice(t * mod_cols, (t + 1) * mod_cols)
-            shift = mod_all[t, which : which + 1, :]
-            scale = mod_all[t, which + 2 : which + 3, :]
-            hidden[at, cols] = (
-                (x[:, cols] * factor) * (1.0 + scale) + shift
-            ).astype(bf16)
+            for k in (0, 1):
+                start = t * mod_cols + k * half_cols
+                cols = slice(start, start + half_cols)
+                shift = mod_all[t, 4 * k + which : 4 * k + which + 1, :]
+                scale = mod_all[t, 4 * k + which + 2 : 4 * k + which + 3, :]
+                hidden[at, cols] = (
+                    (x[:, cols] * factor) * (1.0 + scale) + shift
+                ).astype(bf16)
 
     lane = lax.broadcasted_iota(jnp.int32, (chunk_rows, LANES), 1)
     first_quarter = lane % HEAD_DIM < HEAD_DIM // 2
@@ -855,111 +862,114 @@
             jnp.where(low, pltpu.roll(a, HEAD_DIM, 1), b).astype(bf16),
         )
 
+    core_keys = keys // 2
+
     def kv_at(s, src, core, p):
-        start = (s * 4 + src) * set_rows + core * (tok // 2) + p * pair_rows
+        start = s * keys + core * core_keys + (p * 4 + src) * pair_rows
         return kv_buf.at[pl.ds(pl.multiple_of(start, 16), pair_rows)]
 
     def kvc_at(s, src, core):
-        start = (s * 4 + src) * set_rows + tok + core * (ctx_rows // 2)
+        start = s * keys + core * core_keys + 2 * tok + src * (ctx_rows // 2)
         return kv_buf.at[pl.ds(pl.multiple_of(start, 16), ctx_rows // 2)]
+
+    def kv_block(s, core, p):
+        start = s * keys + core * core_keys + p * 4 * pair_rows
+        size = 2 * ctx_rows if p == pieces else 4 * pair_rows
+        return kv_buf.at[pl.ds(pl.multiple_of(start, 16), size)]
 
     def q_at(s, src, p):
         start = ((s * pieces + p) * 4 + src) * pair_rows
         return pl.ds(pl.multiple_of(start, 16), pair_rows)
 
-    def chunk(s, p, with_ctx):
-        from_partner(s, p)
-        for slot in range(4):
-            modulate(
-                raw[s, slot, p * rows_p : (p + 1) * rows_p, :].astype(f32), 0, slot * rows_p
-            )
-        count = chunk_rows
+    kv_cols = 2 * head_cols + val_cols
+
+    def chunk(s, ps, with_ctx):
+        for i, p in enumerate(ps):
+            from_partner(s, p)
+            start = (s * pieces + p) * chunk_rows
+            modulate(raw[start : start + chunk_rows, :].astype(f32), 0, i * chunk_rows)
+        lat_count = len(ps) * chunk_rows
+        count = lat_count
         if with_ctx:
             if s == 1:
                 from_partner(1, pieces)
-                modulate(far_ctx[...].astype(f32), 1, chunk_rows)
+                modulate(far_ctx[...].astype(f32), 1, lat_count)
             else:
-                modulate(ctx[...].astype(f32), 1, chunk_rows)
-            count = chunk_rows + ctx_rows
-        if s == 0 and p == 0:
-            for load in loads[:5]:
-                load.wait()
-        kv_cols = 2 * head_cols + val_cols
+                modulate(ctx[...].astype(f32), 1, lat_count)
+            count = lat_count + ctx_rows
+        if s == 0 and ps[0] == 0:
+            arrived(w, w_sem.at[0])
         kv = jnp.dot(hidden[:count, :], w[:, :kv_cols], preferred_element_type=f32)
         slabs = [kv[:, m * LANES : (m + 1) * LANES] for m in (0, 1)]
-        pair = pair_up(
-            rope(slabs[0][:chunk_rows], s, p), rope(slabs[1][:chunk_rows], s, p), low_half
-        )
+        vals = [kv[:, (2 + j) * LANES : (3 + j) * LANES].astype(bf16) for j in (0, 1)]
+        for i, p in enumerate(ps):
+            at = slice(i * chunk_rows, (i + 1) * chunk_rows)
+            pair = pair_up(rope(slabs[0][at], s, p), rope(slabs[1][at], s, p), low_half)
+            for j in (0, 1):
+                for core in (0, 1):
+                    rows = slice(core * pair_rows, (core + 1) * pair_rows)
+                    kv_send[s, j, core, p, :, :LANES] = pair[j][rows]
+                    kv_send[s, j, core, p, :, LANES:] = vals[j][at][rows]
         if with_ctx:
-            pair_c = pair_up(slabs[0][chunk_rows:], slabs[1][chunk_rows:], ctx_half)
-        for j in (0, 1):
-            vals = kv[:, (2 + j) * LANES : (3 + j) * LANES].astype(bf16)
-            for core in (0, 1):
-                rows = slice(core * pair_rows, (core + 1) * pair_rows)
-                kv_send[s, j, core, p, :, :LANES] = pair[j][rows]
-                kv_send[s, j, core, p, :, LANES:] = vals[rows]
-            if with_ctx:
-                kvc_send[s, j, :, :LANES] = pair_c[j]
-                kvc_send[s, j, :, LANES:] = vals[chunk_rows:]
+            pair = pair_up(slabs[0][lat_count:], slabs[1][lat_count:], ctx_half)
+            for j in (0, 1):
+                kvc_send[s, j, :, :LANES] = pair[j]
+                kvc_send[s, j, :, LANES:] = vals[j][lat_count:]
         for dj in (1, 0):
             j = (zl_i + dj) % 2
             for dc in (0, 1):
                 core = (c_i + dc) % 2
                 put = send if dj or dc else send_or_keep
+                s_sem = kv_s.at[0] if dj or dc else kv_s.at[1]
                 where = dict(sp=sp_at(half_i, j, c_i), tp=x_i * 2 + core)
-                put(
-                    kv_send.at[s, j, core, p], kv_at(s, src_i, core, p),
-                    kv_s.at[s, p, dj, dc], kv_r.at[s, src_i, p], **where,
-                )
+                for p in ps:
+                    put(
+                        kv_send.at[s, j, core, p], kv_at(s, src_i, core, p),
+                        s_sem, kv_r.at[s, p], **where,
+                    )
                 if with_ctx:
                     half = pl.ds(pl.multiple_of(core * (ctx_rows // 2), 16), ctx_rows // 2)
                     put(
                         kvc_send.at[s, j, half], kvc_at(s, src_i, core),
-                        kvc_s.at[s, dj, dc], kvc_r.at[s, src_i], **where,
+                        s_sem, kv_r.at[s, pieces], **where,
                     )
-        q = jnp.dot(hidden[:chunk_rows, :], w[:, kv_cols:], preferred_element_type=f32)
-        pair = pair_up(rope(q[:, :LANES], s, p), rope(q[:, LANES:], s, p), low_half)
-        for j in (0, 1):
-            for core in (0, 1):
-                q_send[s, j, core, p] = pair[j][core * pair_rows : (core + 1) * pair_rows]
+        q = jnp.dot(hidden[:lat_count, :], w[:, kv_cols:], preferred_element_type=f32)
+        for i, p in enumerate(ps):
+            at = slice(i * chunk_rows, (i + 1) * chunk_rows)
+            pair = pair_up(rope(q[at, :LANES], s, p), rope(q[at, LANES:], s, p), low_half)
+            for j in (0, 1):
+                for core in (0, 1):
+                    q_send[s, j, core, p] = pair[j][core * pair_rows : (core + 1) * pair_rows]
         for dj in (1, 0):
             j = (zl_i + dj) % 2
             for dc in (0, 1):
                 core = (c_i + dc) % 2
                 put = send if dj or dc else send_or_keep
-                put(
-                    q_send.at[s, j, core, p], q_buf.at[q_at(s, src_i, p)],
-                    q_s.at[s, p, dj, dc], q_r.at[s, src_i, p],
-                    sp=sp_at(half_i, j, c_i), tp=x_i * 2 + core,
-                )
-
-    def relay(s, p, with_ctx):
-        for src in range(4):
-            arrived(kv_at(s, src, c_i, p), kv_r.at[s, src, p])
-            send(
-                kv_at(s, src, c_i, p), kv_at(s, src, c_i, p),
-                rel_s.at[s, src, p], rel_r.at[s, src, p], tp=partner,
-            )
-            if with_ctx:
-                arrived(kvc_at(s, src, c_i), kvc_r.at[s, src])
-                send(
-                    kvc_at(s, src, c_i), kvc_at(s, src, c_i),
-                    relc_s.at[s, src], relc_r.at[s, src], tp=partner,
-                )
+                s_sem = q_s.at[0] if dj or dc else q_s.at[1]
+                for p in ps:
+                    put(
+                        q_send.at[s, j, core, p], q_buf.at[q_at(s, src_i, p)],
+                        s_sem, q_r.at[s, p],
+                        sp=sp_at(half_i, j, c_i), tp=x_i * 2 + core,
+                    )
+
+    def relay(s, p):
+        block = kv_block(s, c_i, p)
+        arrived(block, kv_r.at[s, p])
+        send(block, block, kv_s.at[0], rel_r.at[s], tp=partner)
 
     def wait_keys(s):
-        for src in range(4):
-            for p in range(pieces):
-                arrived(kv_at(s, src, 1 - c_i, p), rel_r.at[s, src, p])
-            arrived(kvc_at(s, src, 1 - c_i), relc_r.at[s, src])
+        start = s * keys + (1 - c_i) * core_keys
+        arrived(kv_buf.at[pl.ds(pl.multiple_of(start, 16), core_keys)], rel_r.at[s])
         step = 2 * LANES
         for b in range(keys // step):
             at = s * keys + b * step
             vals_t[s, :, b * step : (b + 1) * step] = kv_buf[at : at + step, LANES:].T
 
     def wait_queries(s, p):
-        for src in range(4):
-            arrived(q_buf.at[q_at(s, src, p)], q_r.at[s, src, p])
+        arrived(
+            q_buf.at[pl.ds((s * pieces + p) * 4 * pair_rows, 4 * pair_rows)], q_r.at[s, p]
+        )
 
     coef = HEAD_DIM ** (-0.5) * 1.4426950408889634
     q_low = lax.broadcasted_iota(jnp.int32, (q_tile, LANES), 1) < HEAD_DIM
@@ -996,6 +1006,9 @@
             mixed * factor * gain_t[:VALUE_DIM, :]
         ).T.astype(bf16)
 
+    def head_row(p, core, h):
+        return ((p * 2 + core) * 4 + h) * pair_rows
+
     def give_back(s, p):
         half = half_i if s == 0 else 1 - half_i
         for dz, dy in mates + [(0, 0)]:
@@ -1003,8 +1016,9 @@
             y = (y_i + dy) % 2
             put = send if s or dz or dy else send_or_keep
             put(
-                o_send.at[q_at(s, zl * 2 + y, p)], heads.at[z_i, c_i, p],
-                o_s.at[s, p, dz * 2 + dy], o_r.at[z_i, c_i, p],
+                o_send.at[q_at(s, zl * 2 + y, p)],
+                heads.at[pl.ds(pl.multiple_of(head_row(p, c_i, z_i), 16), pair_rows)],
+                o_s.at[0] if s or dz or dy else o_s.at[1], o_r.at[p],
                 sp=sp_at(half, zl, y), tp=x_i * 2 + y_i,
             )
 
@@ -1012,12 +1026,16 @@
     part_cols = width // parts
 
     def project(p):
-        for h in range(4):
-            for core in (0, 1):
-                arrived(heads.at[h, core, p], o_r.at[h, core, p])
+        arrived(heads.at[pl.ds(head_row(p, 0, 0), 8 * pair_rows)], o_r.at[p])
         left = jnp.concatenate(
             [
-                jnp.concatenate([heads[h, core, p] for h in range(4)], axis=-1)
+                jnp.concatenate(
+                    [
+                        heads[pl.ds(pl.multiple_of(head_row(p, core, h), 16), pair_rows), :]
+                        for h in range(4)
+                    ],
+                    axis=-1,
+                )
                 for core in (1 - c_i, c_i)
             ],
             axis=0,
@@ -1028,7 +1046,7 @@
             pair_send[p, k] = terms[:pair_rows]
             mine[p, k] = terms[pair_rows:]
             send(
-                pair_send.at[p, k], pair_recv.at[p, k], pair_s.at[p, k], pair_r.at[p, k],
+                pair_send.at[p, k], pair_recv.at[p, k], pair_s.at[0], pair_r.at[p, k],
                 tp=partner,
             )
 
@@ -1040,7 +1058,7 @@
             both = mine[p, k, there, :].astype(f32) + pair_recv[p, k, there, :].astype(f32)
             fin_send[p, k] = both.astype(bf16)
             send(
-                fin_send.at[p, k], fin_recv.at[p, k], fin_s.at[p, k], fin_r.at[p, k], tp=across
+                fin_send.at[p, k], fin_recv.at[p, k], fin_s.at[0], fin_r.at[p, k], tp=across
             )
             own_sum[p, k] = mine[p, k, here, :].astype(f32) + pair_recv[p, k, here, :].astype(f32)
 
@@ -1049,26 +1067,30 @@
         for k in range(parts):
             arrived(fin_recv.at[p, k], fin_r.at[p, k])
             summed = own_sum[p, k] + fin_recv[p, k].astype(f32)
-            done = 0
-            while done < part_cols:
-                col = k * part_cols + done
-                size = min(mod_cols - col % mod_cols, part_cols - done)
-                at = slice(col, col + size)
-                low = col % mod_cols
-                gate = mod_all[col // mod_cols, 4:5, low : low + size]
+            for col in range(0, part_cols, gate_cols):
+                at = slice(k * part_cols + col, k * part_cols + col + gate_cols)
+                block = (k * part_cols + col) // gate_cols
+                gate = gate_all[block // 4, block % 4 : block % 4 + 1, :]
                 out[rows, at] = (
-                    lat[rows, at].astype(f32) + gate * summed[:, done : done + size]
+                    lat[rows, at].astype(f32) + gate * summed[:, col : col + gate_cols]
                 ).astype(bf16)
-                done += size
 
     last = pieces - 1
-    for p in range(last):
-        chunk(0, p, p == 0)
-        if p == 0:
-            from_across(1, pieces)
-    from_far(0)
-    from_across(0, last)
-    chunk(0, last, False)
+    chunk(0, [0], True)
+    @pl.when(jnp.logical_not(outer))
+    def _():
+        send_far(pieces)
+        send_far(0)
+
+    for p in range(1, pieces):
+        from_across(0, p)
+    chunk(0, list(range(1, pieces)), False)
+
+    @pl.when(jnp.logical_not(outer))
+    def _():
+        for p in range(1, pieces):
+            send_far(p)
+
     arrived(par_recv, par_sem.at[1])
     params = jnp.where(owns_head, par_own[...], par_recv[...])
     gain_row = jnp.broadcast_to(params[0:1, :], (VALUE_DIM, VALUE_DIM)).T
@@ -1076,30 +1098,40 @@
     for k in range(q_tile // VALUE_DIM):
         gain_t[:VALUE_DIM, k * VALUE_DIM : (k + 1) * VALUE_DIM] = gain_row
         gain_t[VALUE_DIM:, k * VALUE_DIM : (k + 1) * VALUE_DIM] = lam_row
-    from_across(1, 0)
-    chunk(1, 0, True)
-    for p in range(last):
-        relay(0, p, p == 0)
-    for p in range(1, last):
-        from_far(p)
-        from_across(1, p)
-        chunk(1, p, False)
-    relay(0, last, False)
+    relay(0, 0)
+    relay(0, pieces)
+    for p in range(1, pieces):
+        relay(0, p)
+    from_far(pieces)
+    from_far(0)
+    from_across(1, pieces)
     wait_keys(0)
     for p in range(pieces):
         wait_queries(0, p)
     item(0, 0, True, False)
-    from_far(last)
+    from_across(1, 0)
+    from_far(1)
+    chunk(1, [0], True)
     item(1, 0, True, False)
-    from_across(1, last)
-    chunk(1, last, False)
+    from_across(1, 1)
+    for p in range(2, pieces):
+        from_far(p)
+    chunk(1, [1], False)
+    relay(1, 0)
+    relay(1, pieces)
     item(2, 0, True, False)
-    for p in range(last):
-        relay(1, p, p == 0)
-    for p in range(last):
-        wait_queries(1, p)
-        item(pieces + p, 0, True, False)
-    relay(1, last, False)
+    gate_all[tp_i] = sum_sp(gate_recv, gate_sem)
+    to_all_tp(gate_all, gate_sem)
+    wait_queries(1, 0)
+    item(pieces, 0, True, False)
+    for p in range(2, pieces):
+        from_across(1, p)
+        chunk(1, [p], False)
+    for p in range(1, last):
+        relay(1, p)
+    wait_queries(1, 1)
+    item(pieces + 1, 0, True, False)
+    relay(1, last)
     wait_keys(1)
     wait_queries(1, last)
     for p in range(pieces):
@@ -1112,21 +1144,36 @@
         item(p, 1, False, True)
         give_back(0, p)
         if p == 0:
-            loads[5].wait()
+            arrived(wo, w_sem.at[1])
         else:
             combine(p - 1)
     project(last)
-    for p in range(last):
+    combine(last)
+    arrived(gate_all.at[pl.ds(0, n_tp - 1)], gate_sem.at[3])
+    for p in range(pieces):
         finish(p)
-    combine(last)
-    finish(last)
-    for copy in pending:
-        copy.wait_send()
+    def sent(ref, s_sem):
+        pltpu.make_async_copy(ref, ref, s_sem).wait()
+
+    far_rows = own + ctx_p
+    sent(raw.at[pl.ds(0, 3 * own + 4 * far_rows)], raw_s.at[0])
+    for sems, ref, tp_ref in (
+        (mod_sem, mod_recv, mod_all), (gate_sem, gate_recv, gate_all),
+    ):
+        sent(ref.at[pl.ds(0, n_sp - 1)], sems.at[0])
+        sent(tp_ref.at[pl.ds(0, n_tp - 1)], sems.at[2])
+    sent(par_own, par_sem.at[0])
+    sent(kv_buf.at[pl.ds(0, 3 * set_rows + 2 * core_keys)], kv_s.at[0])
+    sent(q_buf.at[pl.ds(0, 3 * tok)], q_s.at[0])
+    sent(o_send.at[pl.ds(0, 7 * pieces * pair_rows)], o_s.at[0])
+    sent(pair_send, pair_s.at[0])
+    sent(fin_send, fin_s.at[0])
 
     @pl.when(jnp.logical_not(owns_head))
     def _():
-        for copy in when_remote:
-            copy.wait_send()
+        sent(kv_buf.at[pl.ds(0, set_rows)], kv_s.at[1])
+        sent(q_buf.at[pl.ds(0, tok)], q_s.at[1])
+        sent(o_send.at[pl.ds(0, pieces * pair_rows)], o_s.at[1])
 
 
 def split_scratch(n_sp, n_tp, own, width, ctx_rows, mod_cols, groups):
@@ -1142,16 +1189,17 @@
     return [
         pltpu.VMEM((width, 4 * 2 * HEAD_DIM + 2 * VALUE_DIM), bf16),
         pltpu.VMEM((groups * VALUE_DIM, width), bf16),
-        pltpu.VMEM((8, mod_cols), f32),
-        pltpu.VMEM((4, 8, mod_cols), f32),
-        pltpu.VMEM((8, mod_cols), f32),
-        pltpu.VMEM((8, mod_cols), f32),
-        pltpu.VMEM((n_tp, 8, mod_cols), f32),
+        pltpu.VMEM((8, mod_cols // 2), f32),
+        pltpu.VMEM((n_sp, 8, mod_cols // 2), f32),
+        pltpu.VMEM((n_tp, 8, mod_cols // 2), f32),
+        pltpu.VMEM((8, mod_cols // 4), f32),
+        pltpu.VMEM((n_sp, 8, mod_cols // 4), f32),
+        pltpu.VMEM((n_tp, 8, mod_cols // 4), f32),
         pltpu.VMEM((8, VALUE_DIM), f32),
         pltpu.VMEM((8, VALUE_DIM), f32),
-        pltpu.VMEM((2, 4, own, width), bf16),
+        pltpu.VMEM((8 * own, width), bf16),
         pltpu.VMEM((ctx_rows, width), bf16),
-        pltpu.VMEM((2 * pair_rows + ctx_rows, width), bf16),
+        pltpu.VMEM((4 * pair_rows + ctx_rows, width), bf16),
         pltpu.VMEM((2, pieces, 2 * pair_rows, LANES), f32),
         pltpu.VMEM((2, pieces, 2 * pair_rows, LANES), f32),
         pltpu.VMEM((2, 2, 2, pieces, pair_rows, 2 * LANES), bf16),
@@ -1165,41 +1213,31 @@
         pltpu.VMEM((2 * pieces, 8, 2 * q_tile), f32),
         pltpu.VMEM((2 * pieces, VALUE_DIM, 2 * q_tile), f32),
         pltpu.VMEM((2 * pieces * q_tile, LANES), bf16),
-        pltpu.VMEM((4, 2, pieces, pair_rows, LANES), bf16),
+        pltpu.VMEM((8 * pieces * pair_rows, LANES), bf16),
         pltpu.VMEM((pieces, parts, pair_rows, part_cols), bf16),
         pltpu.VMEM((pieces, parts, pair_rows, part_cols), bf16),
         pltpu.VMEM((pieces, parts, pair_rows, part_cols), bf16),
         pltpu.VMEM((pieces, parts, rows_p, part_cols), bf16),
         pltpu.VMEM((pieces, parts, rows_p, part_cols), bf16),
         pltpu.VMEM((pieces, parts, rows_p, part_cols), f32),
-        dma((6,)),
         dma((2,)),
-        dma((3,)),
+        dma((2,)),
         dma((4,)),
-        dma((2,)),
-        dma((n_tp,)),
-        dma((n_tp,)),
-        dma((pieces + 1,)),
+        dma((4,)),
+        dma((1,)),
         dma((pieces + 1,)),
         dma((2, pieces + 1)),
         dma((2, pieces + 1)),
-        dma((2, pieces + 1, 2)),
-        dma((2, pieces + 1, 2)),
-        dma((2, pieces, 2, 2)),
-        dma((2, 4, pieces)),
-        dma((2, 2, 2)),
-        dma((2, 4)),
-        dma((2, pieces, 2, 2)),
-        dma((2, 4, pieces)),
-        dma((2, 4, pieces)),
-        dma((2, 4, pieces)),
-        dma((2, 4)),
-        dma((2, 4)),
-        dma((2, pieces, 4)),
-        dma((4, 2, pieces)),
+        dma((2,)),
+        dma((2, pieces + 1)),
+        dma((2,)),
+        dma((2,)),
+        dma((2, pieces)),
+        dma((2,)),
+        dma((pieces,)),
+        dma((1,)),
         dma((pieces, parts)),
-        dma((pieces, parts)),
-        dma((pieces, parts)),
+        dma((1,)),
         dma((pieces, parts)),
     ]
 

time: 90.1 us -> 78.3 us (0.87)
  Pallas kernels: 88.1 us -> 76.4 us
    pallas_call x1, Pallas kernels: 88.1 us -> 76.4 us  [local(): pl.pallas_call(functools.partial(kernel, n_sp, n_tp), out_shape=jax.Shape...]
where the time goes in v2:
time: 78.3 us; the launch traced here: 78.2 us
  Pallas kernels  76.4 us (98%)
  local copies, waits for them, and re-layouts  1.77 us (2%)
    pallas_call x1, Pallas kernels, local(): pl.pallas_call(functools.partial(kernel, n_sp, n_tp), out_shape=jax.Shape...  76.4 us
    unnamed x1, local copies, waits for them, and re-layouts  1.77 us

profile of v2, /device:TPU:0, one launch (start us, length us, event | category | flops | bytes accessed | tf_op | source)
XLA Modules:
  0.0 78.2 jit_solution(8010820910487080733)
XLA Ops:
  0.0 76.4 %diff_attention.1 = bf16[96,2048]{1,0:T(8,128)(2,1)} custom-call(bf16[96,2048]{1,0:T(8,128)(2,1)} %lat.1, bf16[64,2048]{1,0:T(8,128)(2,1)} %ctx.1, f32[8,1,256]{2,1,0:T(1,128)} %bitcast.3, f32[8,1,256]{2,1,0:T(1,128)} %bitcast.4, bf16[256,512]{1,0:T(8,128)(2,1)} %shift_w.1, bf16[256,512]{1,0:T(8,128)(2,1)} %scale_w.1, bf16[256,512]{1,0:T(8,128)(2,1)} %gate_w.1, ...), custom_call_target="tpu_custom_call" | custom-call | tf_op jit(solution)/shard_map/diff_attention/pallas_call | solution.py:1344
  76.4 1.8 %copy.16 = bf16[96,2048]{1,0:T(8,128)(2,1)} copy(bf16[96,2048]{1,0:T(8,128)(2,1)} %diff_attention.1) | data formatting | bytes 786432

commit v3 on v2

--- a/solution.py
+++ b/solution.py
@@ -530,6 +530,21 @@
 def split_body(
     n_sp,
     n_tp,
+    lat_hbm,
+    ctx_hbm,
+    cond_l_hbm,
+    cond_c_hbm,
+    shift_hbm,
+    scale_hbm,
+    gate_hbm,
+    lane_table_hbm,
+    lam,
+    gain_hbm,
+    wq_hbm,
+    wk_hbm,
+    wv_hbm,
+    wo_hbm,
+    out,
     lat,
     ctx,
     cond_l,
@@ -538,13 +553,7 @@
     scale_w,
     gate_w,
     lane_table,
-    lam,
     gain,
-    wq_hbm,
-    wk_hbm,
-    wv_hbm,
-    wo_hbm,
-    out,
     w,
     wo,
     mod_part,
@@ -578,6 +587,7 @@
     fin_send,
     fin_recv,
     own_sum,
+    in_sem,
     w_sem,
     par_sem,
     mod_sem,
@@ -651,6 +661,19 @@
     def sp_at(half, zl, y):
         return (half * 2 + zl) * 2 + y
 
+    staged = [
+        pltpu.make_async_copy(a, b, in_sem.at[i])
+        for i, (a, b) in enumerate(
+            (
+                (cond_l_hbm, cond_l), (cond_c_hbm, cond_c), (shift_hbm, shift_w),
+                (scale_hbm, scale_w), (gain_hbm, gain), (lat_hbm, lat), (ctx_hbm, ctx),
+                (gate_hbm, gate_w), (lane_table_hbm, lane_table),
+            )
+        )
+    ]
+    for copy in staged:
+        copy.start()
+
     head_cols = 2 * HEAD_DIM
     val_cols = 2 * VALUE_DIM
 
@@ -674,8 +697,6 @@
         )
     loads = [pltpu.make_async_copy(a, b, w_sem.at[0]) for a, b in loads]
     loads.append(pltpu.make_async_copy(wo_hbm, wo, w_sem.at[1]))
-    for load in loads:
-        load.start()
 
     barrier = pltpu.get_barrier_semaphore()
     for k in range(1, n_sp):
@@ -688,6 +709,11 @@
         pl.semaphore_signal(
             barrier, inc=1, device_id={"tp": (tp_i + k) % n_tp}, device_id_type=MESH
         )
+
+    for load in loads:
+        load.start()
+    for copy in staged[:5]:
+        copy.wait()
 
     def silu(v):
         return (v / (1.0 + jnp.exp(-v))).astype(bf16).astype(f32)
@@ -715,6 +741,8 @@
     mod_part[...] = mod_total
     par_own[0:1, :] = gain[z_i]
     par_own[1:2, :] = jnp.full((1, VALUE_DIM), lam[z_i], f32)
+    for copy in staged[5:]:
+        copy.wait()
     pl.semaphore_wait(barrier, 2 * (n_sp - 1) + n_tp - 1)
 
     def to_all_sp(src, dst, sems):
@@ -776,6 +804,9 @@
         slot = c_i * 2 + (1 - x_i)
         arrived(piece(s, slot, p), x_r.at[s, p])
         send(piece(s, slot, p), piece(s, slot, p), raw_s.at[0], d_r.at[s, p], tp=partner)
+
+    def from_across_far(p):
+        from_across(1, p)
 
     def from_partner(s, p):
         arrived(piece_pair(s, 1 - c_i, p), d_r.at[s, p])
@@ -816,14 +847,16 @@
 
     mod_all[tp_i] = sum_sp(mod_recv, mod_sem)
     to_all_tp(mod_all, mod_sem)
-    outer = zl_i != half_i
-
-    @pl.when(outer)
-    def _():
-        send_far(pieces)
-        for p in range(pieces):
-            send_far(p)
-
+    inner = zl_i != half_i
+    outer = jnp.logical_not(inner)
+
+    def at(condition, action, *ps):
+        @pl.when(condition)
+        def _():
+            for p in ps:
+                action(p)
+
+    at(inner, send_far, pieces, *range(pieces))
     for p in range(1, pieces):
         spread_x(0, p)
     to_all_sp(gate_part, gate_recv, gate_sem)
@@ -1041,8 +1074,10 @@
             axis=0,
         )
         for k in range(parts):
-            at = slice(k * part_cols, (k + 1) * part_cols)
-            terms = jnp.dot(left, wo[:, at], preferred_element_type=f32).astype(bf16)
+            if k % 2 == 0:
+                at = slice(k * part_cols, (k + 2) * part_cols)
+                both = jnp.dot(left, wo[:, at], preferred_element_type=f32).astype(bf16)
+            terms = both[:, k % 2 * part_cols : (k % 2 + 1) * part_cols]
             pair_send[p, k] = terms[:pair_rows]
             mine[p, k] = terms[pair_rows:]
             send(
@@ -1077,20 +1112,12 @@
 
     last = pieces - 1
     chunk(0, [0], True)
-    @pl.when(jnp.logical_not(outer))
-    def _():
-        send_far(pieces)
-        send_far(0)
-
+    at(outer, send_far, pieces, 0)
     for p in range(1, pieces):
         from_across(0, p)
+    at(outer, from_far, pieces, 0)
     chunk(0, list(range(1, pieces)), False)
-
-    @pl.when(jnp.logical_not(outer))
-    def _():
-        for p in range(1, pieces):
-            send_far(p)
-
+    at(outer, send_far, *range(1, pieces))
     arrived(par_recv, par_sem.at[1])
     params = jnp.where(owns_head, par_own[...], par_recv[...])
     gain_row = jnp.broadcast_to(params[0:1, :], (VALUE_DIM, VALUE_DIM)).T
@@ -1098,54 +1125,56 @@
     for k in range(q_tile // VALUE_DIM):
         gain_t[:VALUE_DIM, k * VALUE_DIM : (k + 1) * VALUE_DIM] = gain_row
         gain_t[VALUE_DIM:, k * VALUE_DIM : (k + 1) * VALUE_DIM] = lam_row
+    at(outer, from_far, 1)
     relay(0, 0)
     relay(0, pieces)
+    at(inner, from_far, pieces, 0)
     for p in range(1, pieces):
         relay(0, p)
-    from_far(pieces)
-    from_far(0)
     from_across(1, pieces)
     wait_keys(0)
     for p in range(pieces):
         wait_queries(0, p)
     item(0, 0, True, False)
-    from_across(1, 0)
-    from_far(1)
+    at(outer, from_across_far, 0)
+    item(1, 0, True, False)
+    at(inner, from_across_far, 0)
+    at(inner, from_far, 1)
+    at(outer, from_far, *range(2, pieces))
     chunk(1, [0], True)
-    item(1, 0, True, False)
+    at(inner, from_far, *range(2, pieces))
     from_across(1, 1)
+    chunk(1, [1], False)
     for p in range(2, pieces):
-        from_far(p)
-    chunk(1, [1], False)
+        from_across(1, p)
+    item(2, 0, True, False)
+    for p in range(2, pieces):
+        chunk(1, [p], False)
     relay(1, 0)
     relay(1, pieces)
-    item(2, 0, True, False)
+    for p in range(1, last):
+        relay(1, p)
     gate_all[tp_i] = sum_sp(gate_recv, gate_sem)
     to_all_tp(gate_all, gate_sem)
-    wait_queries(1, 0)
-    item(pieces, 0, True, False)
-    for p in range(2, pieces):
-        from_across(1, p)
-        chunk(1, [p], False)
-    for p in range(1, last):
-        relay(1, p)
-    wait_queries(1, 1)
-    item(pieces + 1, 0, True, False)
+    for p in range(last):
+        wait_queries(1, p)
+        item(pieces + p, 0, True, False)
     relay(1, last)
+    wait_queries(1, last)
+    item(pieces + last, 0, True, False)
     wait_keys(1)
-    wait_queries(1, last)
+    arrived(wo, w_sem.at[1])
     for p in range(pieces):
-        if p == last:
-            item(pieces + p, 0, True, False)
         item(pieces + p, 1, False, True)
         give_back(1, p)
-        if p > 0:
+        if p == last:
             project(p - 1)
         item(p, 1, False, True)
         give_back(0, p)
-        if p == 0:
-            arrived(wo, w_sem.at[1])
-        else:
+        if p == last:
+            combine(p - 1)
+        elif p > 0:
+            project(p - 1)
             combine(p - 1)
     project(last)
     combine(last)
@@ -1176,17 +1205,26 @@
         sent(o_send.at[pl.ds(0, pieces * pair_rows)], o_s.at[1])
 
 
-def split_scratch(n_sp, n_tp, own, width, ctx_rows, mod_cols, groups):
+def split_scratch(n_sp, n_tp, own, width, ctx_rows, mod_rows, mod_cols, groups):
     tok = own * n_tp
     pieces = 3
     rows_p = own // pieces
     pair_rows = 2 * rows_p
     q_tile = 4 * pair_rows
     keys = 4 * (tok + ctx_rows)
-    parts = 2
+    parts = 4
     part_cols = width // parts
     dma = pltpu.SemaphoreType.DMA
     return [
+        pltpu.VMEM((own, width), bf16),
+        pltpu.VMEM((ctx_rows, width), bf16),
+        pltpu.VMEM((n_sp, 1, mod_rows), f32),
+        pltpu.VMEM((n_sp, 1, mod_rows), f32),
+        pltpu.VMEM((mod_rows, mod_cols), bf16),
+        pltpu.VMEM((mod_rows, mod_cols), bf16),
+        pltpu.VMEM((mod_rows, mod_cols), bf16),
+        pltpu.VMEM((8, LANES), f32),
+        pltpu.VMEM((groups, 1, VALUE_DIM), f32),
         pltpu.VMEM((width, 4 * 2 * HEAD_DIM + 2 * VALUE_DIM), bf16),
         pltpu.VMEM((groups * VALUE_DIM, width), bf16),
         pltpu.VMEM((8, mod_cols // 2), f32),
@@ -1220,6 +1258,7 @@
         pltpu.VMEM((pieces, parts, rows_p, part_cols), bf16),
         pltpu.VMEM((pieces, parts, rows_p, part_cols), bf16),
         pltpu.VMEM((pieces, parts, rows_p, part_cols), f32),
+        dma((9,)),
         dma((2,)),
         dma((2,)),
         dma((4,)),
@@ -1336,15 +1375,16 @@
         dma((chips, parts)),
         dma((chips, parts)),
     ]
-    kernel = body
+    kernel, staged = body, vmem
     fits = own % 48 == 0 and ctx_rows % (16 * n_tp) == 0 and own * 8 // 3 % LANES == 0
     if (n_sp, n_tp, groups) == (8, 4, 4) and fits and (tok + ctx_rows) % 64 == 0:
         kernel = split_body
-        scratch = split_scratch(n_sp, n_tp, own, width, ctx_rows, mod_cols, groups)
+        scratch = split_scratch(n_sp, n_tp, own, width, ctx_rows, mod_rows, mod_cols, groups)
+        staged = hbm
     return pl.pallas_call(
         functools.partial(kernel, n_sp, n_tp),
         out_shape=jax.ShapeDtypeStruct((own, width), bf16),
-        in_specs=[vmem] * 8 + [pl.BlockSpec(memory_space=pltpu.SMEM), vmem] + [hbm] * 4,
+        in_specs=[staged] * 8 + [pl.BlockSpec(memory_space=pltpu.SMEM), staged] + [hbm] * 4,
         out_specs=vmem,
         scratch_shapes=scratch,
         compiler_params=pltpu.CompilerParams(

time: 78.3 us -> 74.4 us (0.950)
  Pallas kernels: 76.4 us -> 72.4 us
    pallas_call x1, Pallas kernels: 76.4 us -> 72.4 us  [local(): pl.pallas_call(functools.partial(kernel, n_sp, n_tp), out_shape=jax.Shape...]
where the time goes in v3:
time: 74.4 us; the launch traced here: 74.2 us
  Pallas kernels  72.4 us (97%)
  local copies, waits for them, and re-layouts  1.77 us (2%)
    pallas_call x1, Pallas kernels, local(): pl.pallas_call(functools.partial(kernel, n_sp, n_tp), out_shape=jax.Shape...  72.4 us
    unnamed x1, local copies, waits for them, and re-layouts  1.77 us

profile of v3, /device:TPU:0, one launch (start us, length us, event | category | flops | bytes accessed | tf_op | source)
XLA Modules:
  0.0 74.2 jit_solution(13809994045793502187)
XLA Ops:
  0.0 72.4 %diff_attention.1 = bf16[96,2048]{1,0:T(8,128)(2,1)} custom-call(bf16[96,2048]{1,0:T(8,128)(2,1)} %lat_hbm.1, bf16[64,2048]{1,0:T(8,128)(2,1)} %ctx_hbm.1, f32[8,1,256]{2,1,0:T(1,128)} %bitcast.3, f32[8,1,256]{2,1,0:T(1,128)} %bitcast.4, bf16[256,512]{1,0:T(8,128)(2,1)} %shift_hbm.1, bf16[256,512]{1,0:T(8,128)(2,1)} %scale_hbm.1, bf16[256,512]{1,0:T(8,128)(2,1)} %gate_hbm.1, ...), custom_call_target="tpu_custom_call" | custom-call | tf_op jit(solution)/shard_map/diff_attention/pallas_call | solution.py:1384
  72.4 1.8 %copy.16 = bf16[96,2048]{1,0:T(8,128)(2,1)} copy(bf16[96,2048]{1,0:T(8,128)(2,1)} %diff_attention.1) | data formatting | bytes 786432

commit v4 on v3

--- a/solution.py
+++ b/solution.py
@@ -1131,11 +1131,11 @@
     at(inner, from_far, pieces, 0)
     for p in range(1, pieces):
         relay(0, p)
-    from_across(1, pieces)
     wait_keys(0)
     for p in range(pieces):
         wait_queries(0, p)
     item(0, 0, True, False)
+    from_across(1, pieces)
     at(outer, from_across_far, 0)
     item(1, 0, True, False)
     at(inner, from_across_far, 0)
@@ -1168,6 +1168,8 @@
         item(pieces + p, 1, False, True)
         give_back(1, p)
         if p == last:
+            if p > 1:
+                combine(p - 2)
             project(p - 1)
         item(p, 1, False, True)
         give_back(0, p)
@@ -1175,7 +1177,8 @@
             combine(p - 1)
         elif p > 0:
             project(p - 1)
-            combine(p - 1)
+            if p < last - 1:
+                combine(p - 1)
     project(last)
     combine(last)
     arrived(gate_all.at[pl.ds(0, n_tp - 1)], gate_sem.at[3])

time: 74.4 us -> 73.7 us (level)
  no operation moved by 1% of the time
where the time goes in v4:
time: 73.7 us; the launch traced here: 73.5 us
  Pallas kernels  71.7 us (97%)
  local copies, waits for them, and re-layouts  1.77 us (2%)
    pallas_call x1, Pallas kernels, local(): pl.pallas_call(functools.partial(kernel, n_sp, n_tp), out_shape=jax.Shape...  71.7 us
    unnamed x1, local copies, waits for them, and re-layouts  1.77 us

profile of v4, /device:TPU:0, one launch (start us, length us, event | category | flops | bytes accessed | tf_op | source)
XLA Modules:
  0.0 73.5 jit_solution(8890721621732531405)
XLA Ops:
  0.0 71.7 %diff_attention.1 = bf16[96,2048]{1,0:T(8,128)(2,1)} custom-call(bf16[96,2048]{1,0:T(8,128)(2,1)} %lat_hbm.1, bf16[64,2048]{1,0:T(8,128)(2,1)} %ctx_hbm.1, f32[8,1,256]{2,1,0:T(1,128)} %bitcast.3, f32[8,1,256]{2,1,0:T(1,128)} %bitcast.4, bf16[256,512]{1,0:T(8,128)(2,1)} %shift_hbm.1, bf16[256,512]{1,0:T(8,128)(2,1)} %scale_hbm.1, bf16[256,512]{1,0:T(8,128)(2,1)} %gate_hbm.1, ...), custom_call_target="tpu_custom_call" | custom-call | tf_op jit(solution)/shard_map/diff_attention/pallas_call | solution.py:1387
  71.7 1.8 %copy.16 = bf16[96,2048]{1,0:T(8,128)(2,1)} copy(bf16[96,2048]{1,0:T(8,128)(2,1)} %diff_attention.1) | data formatting | bytes 786432
